TPU v7x, 512 devices: a 4x2x32 block of a 4x8x32 slice. The times are simulated.
512 devices in a mesh: grp: 2 (over y), tp: 32 (over z), dp: 8 (over x, core).
Axes of the slice: x: 4, y: 2, z: 32, core: 2. Of those that a mesh axis runs over, the one named last changes fastest.
The devices are a block of a 4x8x32 slice.
Arguments:
- hidden_in: bfloat16 [192, 4096], P(('grp', 'tp'), 'dp'), parts along dimension 0, may hold values from -40 to 40
- input_norm_gain: float32 [2, 4096], P(None, 'dp'), may hold values from 0.1 to 1.9
- w_query: bfloat16 [2, 4096, 2048], P(None, 'dp', 'tp'), may hold values from -0.09375 to 0.09375
- w_key: bfloat16 [2, 4096, 2048], P(None, 'dp', 'tp'), may hold values from -0.09375 to 0.09375
- w_decay: bfloat16 [2, 4096, 2048], P(None, 'dp', 'tp'), may hold values from -0.375 to 0.375
- w_value: bfloat16 [2, 4096, 4096], P(None, 'dp', 'tp'), may hold values from -0.09375 to 0.09375
- w_gate: bfloat16 [2, 4096, 4096], P(None, 'dp', 'tp'), may hold values from -0.09375 to 0.09375
- out_gain: float32 [2, 4096], P(None, 'tp'), may hold values from 0.1 to 1.9
- w_out: bfloat16 [2, 4096, 4096], P(None, 'tp', 'dp'), may hold values from -0.09375 to 0.09375
- decay_offset: float32 [2, 192, 2048], P(None, ('grp', 'dp'), 'tp'), parts along dimension 1, may hold values from -0.7 to 0
- state: float32 [2, 192, 32, 64, 128], P(None, ('grp', 'dp'), 'tp'), parts along dimension 1, may hold values from -3 to 3
Outputs:
- hidden_out: bfloat16 [192, 4096], P(('grp', 'tp'), 'dp'), parts along dimension 0
- new_state: float32 [2, 192, 32, 64, 128], P(None, ('grp', 'dp'), 'tp'), parts along dimension 1
There are 2 independent parts, one for each index of `grp`. A program takes and returns all parts, laid end to end along the dimension named above; an argument that names none is the same for every part. Nothing has to cross between parts.
All inputs are finite; a program needn't handle non-finite values.
Results may differ from a plain program's by a relative error of at most 0.017.
Values may be sent and summed in bfloat16 or wider, within the bound.
No kernel may reach another device: no remote copies, remote signals or barrier semaphores. Data moves between devices by JAX's collectives and lax.ppermute only.
A program may use at most 64 MiB of HBM per device.

v0:
```python
import jax
import jax.numpy as jnp
from jax import lax
from jax.sharding import PartitionSpec as P

D = 4096
HEAD_KEY = 64
VALUE_CHANNELS = 128
LAYERS = 2


epsilon = 1e-06
softness_factor = 16.0


def in_blocks(value, dim, length):
    lengths = value.shape
    blocks = value.reshape(*lengths[:dim], length, lengths[dim] // length, *lengths[dim + 1 :])
    return jnp.moveaxis(blocks, dim, 0)


def summed_on_arrival(value, axis, dim):
    blocks = in_blocks(value, dim, lax.axis_size(axis))
    arrived = lax.all_to_all(blocks, axis, split_axis=0, concat_axis=0, tiled=True)
    return arrived.astype(jnp.float32).sum(axis=0)


def copy_for_each(value, axis):
    length = lax.axis_size(axis)
    return lax.all_to_all(
        jnp.broadcast_to(value[None], (length, *value.shape)), axis, 0, 0, tiled=True
    )


def joined_along(blocks, dim):
    lengths = list(blocks.shape[1:])
    lengths[dim] *= blocks.shape[0]
    return jnp.moveaxis(blocks, 0, dim).reshape(lengths)


def gathered_copies(value, axis, dim):
    blocks = copy_for_each(value, axis)
    return joined_along(blocks, dim)


def of_everyone(value, axis):
    everything = copy_for_each(value, axis)
    return jnp.sum(everything, axis=0)


def split_heads_sum(head_terms, current):
    own_part = summed_on_arrival(head_terms.astype(jnp.bfloat16), "tp", 0)
    return (current.astype(jnp.float32) + own_part).astype(jnp.bfloat16)


def per_device(
    hidden_in,
    input_norm_gain,
    w_query,
    w_key,
    w_decay,
    w_value,
    w_gate,
    out_gain,
    w_out,
    decay_offset,
    state,
):
    seq_rows = state.shape[1]
    local_heads = state.shape[2]
    key_cols = local_heads * HEAD_KEY
    value_cols = local_heads * VALUE_CHANNELS
    seq_start = lax.axis_index("dp") * seq_rows
    current = hidden_in
    gathered = None
    states = []
    for index_of_block in range(LAYERS):
        gathered = gathered_copies(current, "tp", 0)
        widened = gathered.astype(jnp.float32)
        squares = jnp.sum(widened * widened, axis=1)
        scaled_query = (widened * input_norm_gain[index_of_block][None, :]).astype(jnp.bfloat16)
        partial_value = jnp.concatenate(
            [
                jnp.dot(scaled_query, matrix[index_of_block], preferred_element_type=jnp.float32)
                for matrix in (w_query, w_key, w_decay, w_value, w_gate)
            ],
            axis=1,
        ).astype(jnp.bfloat16)
        summed = summed_on_arrival(partial_value, "dp", 0)
        whole_squares = of_everyone(squares, "dp")
        own_squares = lax.dynamic_slice_in_dim(whole_squares, seq_start, seq_rows)
        inverse = lax.rsqrt(own_squares / D + epsilon)[:, None]
        projected = summed * inverse
        query_rows = projected[:, :key_cols].reshape(seq_rows, local_heads, HEAD_KEY)
        key_rows = projected[:, key_cols : 2 * key_cols].reshape(
            seq_rows, local_heads, HEAD_KEY
        ) * HEAD_KEY ** (-0.5)
        decay_logits = projected[:, 2 * key_cols : 3 * key_cols]
        value_rows = projected[:, 3 * key_cols : 3 * key_cols + value_cols].reshape(
            seq_rows, local_heads, VALUE_CHANNELS
        )
        gate_rows = projected[:, 3 * key_cols + value_cols :].reshape(
            seq_rows, local_heads, VALUE_CHANNELS
        )
        decay_logarithm = (
            jax.nn.log_sigmoid(decay_logits) / softness_factor + decay_offset[index_of_block]
        )
        decay_rate = jnp.exp(decay_logarithm).reshape(seq_rows, local_heads, HEAD_KEY)
        fresh = (
            decay_rate[:, :, :, None] * state[index_of_block]
            + key_rows[:, :, :, None] * value_rows[:, :, None, :]
        )
        readout = jnp.sum(query_rows[:, :, :, None] * fresh, axis=2)
        normed = readout * lax.rsqrt(jnp.mean(readout * readout, axis=2, keepdims=True) + epsilon)
        normed = normed * out_gain[index_of_block].reshape(local_heads, VALUE_CHANNELS)[None]
        gated_out = (
            (normed * jax.nn.silu(gate_rows)).reshape(seq_rows, value_cols).astype(jnp.bfloat16)
        )
        out_matrix = w_out[index_of_block]
        head_terms = jnp.dot(
            gathered_copies(gated_out, "dp", 0), out_matrix, preferred_element_type=jnp.float32
        )
        current = split_heads_sum(head_terms, current)
        gathered = None
        states.append(fresh)
    return (current, jnp.stack(states))


def solution(mesh):
    return jax.shard_map(
        per_device,
        mesh=mesh,
        in_specs=(
            P(("grp", "tp"), "dp"),
            P(None, "dp"),
            P(None, "dp", "tp"),
            P(None, "dp", "tp"),
            P(None, "dp", "tp"),
            P(None, "dp", "tp"),
            P(None, "dp", "tp"),
            P(None, "tp"),
            P(None, "tp", "dp"),
            P(None, ("grp", "dp"), "tp"),
            P(None, ("grp", "dp"), "tp", None, None),
        ),
        out_specs=(P(("grp", "tp"), "dp"), P(None, ("grp", "dp"), "tp", None, None)),
        check_vma=False,
    )
```

profile of v0, /device:TPU:40, one launch (start us, length us, event | category | flops | bytes accessed | tf_op | source)
XLA Modules:
  0.0 242.7 jit_solution(2516870819133110794)
XLA Ops:
  0.6 1.4 broadcast_in_dim.16
  2.0 45.9 %all-to-all-start = ((bf16[32,3,512]{2,1,0:T(4,128)(2,1)}), bf16[32,3,512]{2,1,0:T(4,128)(2,1)S(1)}, u32[]{:S(2)}, u32[]{:S(2)}) async-start(bf16[32,3,512]{2,1,0:T(4,128)(2,1)} %broadcast_in_dim.16), calls=%async_computation | async-start | bytes 262144 | tf_op jit(solution)/shard_map/all_to_all | solution.py:30
  47.9 0.7 copy-done.10
  48.7 30.2 %all-to-all-done = bf16[32,3,512]{2,1,0:T(4,128)(2,1)S(1)} async-done(((bf16[32,3,512]{2,1,0:T(4,128)(2,1)}), bf16[32,3,512]{2,1,0:T(4,128)(2,1)S(1)}, u32[]{:S(2)}, u32[]{:S(2)}) %all-to-all-start) | async-done | bytes 98336 | tf_op jit(solution)/shard_map/all_to_all | solution.py:30
  79.1 0.6 broadcast_in_dim.18
  79.7 4.6 %all-to-all-start.2 = ((f32[8,1,96]{2,1,0:T(1,128)}), f32[8,1,96]{2,1,0:T(1,128)S(1)}, u32[]{:S(2)}, u32[]{:S(2)}) async-start(f32[8,1,96]{2,1,0:T(1,128)} %broadcast_in_dim.18), calls=%async_computation.2 | async-start | bytes 8192 | tf_op jit(solution)/shard_map/all_to_all | solution.py:30
  84.6 0.7 copy-done.2
  85.4 0.7 copy-done.4
  86.7 0.8 concatenate.10
  87.5 2.0 all-to-all-done.2
  89.5 3.6 %all-to-all-start.1 = ((bf16[8,12,448]{2,1,0:T(8,128)(2,1)}), bf16[8,12,448]{2,1,0:T(8,128)(2,1)S(1)}, u32[]{:S(2)}, u32[]{:S(2)}) async-start(bf16[8,12,448]{2,1,0:T(8,128)(2,1)} %concatenate.10), calls=%async_computation.1 | async-start | bytes 262144 | tf_op jit(solution)/shard_map/all_to_all | solution.py:24
  93.2 5.8 %all-to-all-done.1 = bf16[8,12,448]{2,1,0:T(8,128)(2,1)S(1)} async-done(((bf16[8,12,448]{2,1,0:T(8,128)(2,1)}), bf16[8,12,448]{2,1,0:T(8,128)(2,1)S(1)}, u32[]{:S(2)}, u32[]{:S(2)}) %all-to-all-start.1) | async-done | bytes 86048 | tf_op jit(solution)/shard_map/all_to_all | solution.py:24
  99.2 0.4 fusion.5
  99.9 7.9 %all_to_all.52 = bf16[8,12,128]{2,1,0:T(8,128)(2,1)S(1)} all-to-all(bf16[8,12,128]{2,1,0:T(8,128)(2,1)S(1)} %broadcast_in_dim.19), channel_id=1, replica_groups=mesh['grp'=2,'tp'=32,'dp'=8] {'dp'}, dimensions={0} | all-to-all | bytes 49152 | tf_op jit(solution)/shard_map/all_to_all | solution.py:30
  108.0 34.9 %all_to_all.53 = bf16[32,3,512]{2,1,0:T(4,128)(2,1)S(1)} all-to-all(bf16[32,3,512]{2,1,0:T(4,128)(2,1)S(1)} %reshape.295), channel_id=1, replica_groups=mesh['grp'=2,'tp'=32,'dp'=8] {'tp'}, dimensions={0} | all-to-all | bytes 196608 | tf_op jit(solution)/shard_map/all_to_all | solution.py:24
  143.0 0.6 copy-done.7
  143.6 33.3 %all_to_all.54 = bf16[32,3,512]{2,1,0:T(4,128)(2,1)S(1)} all-to-all(bf16[32,3,512]{2,1,0:T(4,128)(2,1)S(1)} %broadcast_in_dim.20), channel_id=1, replica_groups=mesh['grp'=2,'tp'=32,'dp'=8] {'tp'}, dimensions={0} | all-to-all | bytes 196608 | tf_op jit(solution)/shard_map/all_to_all | solution.py:30
  176.9 0.2 fusion.9
  178.0 0.6 broadcast_in_dim.22
  178.6 3.5 %all-to-all-start.7 = ((f32[8,1,96]{2,1,0:T(1,128)}), f32[8,1,96]{2,1,0:T(1,128)S(1)}, u32[]{:S(2)}, u32[]{:S(2)}) async-start(f32[8,1,96]{2,1,0:T(1,128)} %broadcast_in_dim.22), calls=%async_computation.7 | async-start | bytes 8192 | tf_op jit(solution)/shard_map/all_to_all | solution.py:30
  182.3 0.8 concatenate.11
  183.1 4.0 %all-to-all-done.7 = f32[8,1,96]{2,1,0:T(1,128)S(1)} async-done(((f32[8,1,96]{2,1,0:T(1,128)}), f32[8,1,96]{2,1,0:T(1,128)S(1)}, u32[]{:S(2)}, u32[]{:S(2)}) %all-to-all-start.7) | async-done | bytes 3104 | tf_op jit(solution)/shard_map/all_to_all | solution.py:30
  187.1 3.6 %all-to-all-start.6 = ((bf16[8,12,448]{2,1,0:T(8,128)(2,1)}), bf16[8,12,448]{2,1,0:T(8,128)(2,1)S(1)}, u32[]{:S(2)}, u32[]{:S(2)}) async-start(bf16[8,12,448]{2,1,0:T(8,128)(2,1)} %concatenate.11), calls=%async_computation.6 | async-start | bytes 262144 | tf_op jit(solution)/shard_map/all_to_all | solution.py:24
  190.8 5.8 %all-to-all-done.6 = bf16[8,12,448]{2,1,0:T(8,128)(2,1)S(1)} async-done(((bf16[8,12,448]{2,1,0:T(8,128)(2,1)}), bf16[8,12,448]{2,1,0:T(8,128)(2,1)S(1)}, u32[]{:S(2)}, u32[]{:S(2)}) %all-to-all-start.6) | async-done | bytes 86048 | tf_op jit(solution)/shard_map/all_to_all | solution.py:24
  196.8 0.4 fusion.2
  197.5 7.9 %all_to_all.55 = bf16[8,12,128]{2,1,0:T(8,128)(2,1)S(1)} all-to-all(bf16[8,12,128]{2,1,0:T(8,128)(2,1)S(1)} %broadcast_in_dim.23), channel_id=1, replica_groups=mesh['grp'=2,'tp'=32,'dp'=8] {'dp'}, dimensions={0} | all-to-all | bytes 49152 | tf_op jit(solution)/shard_map/all_to_all | solution.py:30
  205.5 0.7 reshape.297
  206.2 4.8 %all-to-all-start.9 = ((bf16[32,3,512]{2,1,0:T(4,128)(2,1)}), bf16[32,3,512]{2,1,0:T(4,128)(2,1)S(1)}, u32[]{:S(2)}, u32[]{:S(2)}) async-start(bf16[32,3,512]{2,1,0:T(4,128)(2,1)} %reshape.297), calls=%async_computation.9 | async-start | bytes 262144 | tf_op jit(solution)/shard_map/all_to_all | solution.py:24
  211.0 0.5 multiply_add_fusion.1
  211.5 0.9 pad_maximum_fusion
  212.4 29.6 %all-to-all-done.9 = bf16[32,3,512]{2,1,0:T(4,128)(2,1)S(1)} async-done(((bf16[32,3,512]{2,1,0:T(4,128)(2,1)}), bf16[32,3,512]{2,1,0:T(4,128)(2,1)S(1)}, u32[]{:S(2)}, u32[]{:S(2)}) %all-to-all-start.9) | async-done | bytes 98336 | tf_op jit(solution)/shard_map/all_to_all | solution.py:24
  242.1 0.6 add_convert_fusion
  (65 shorter events, 4.0 us)
Async XLA Ops:
  2.0 46.6 %copy-start.9 = (f32[2,512]{1,0:T(2,128)S(1)}, f32[2,512]{1,0:T(2,128)}, u32[]{:S(2)}) copy-start(f32[2,512]{1,0:T(2,128)} %param.12) | copy-start | bytes 12292
  2.0 76.8 %all-to-all-start = ((bf16[32,3,512]{2,1,0:T(4,128)(2,1)}), bf16[32,3,512]{2,1,0:T(4,128)(2,1)S(1)}, u32[]{:S(2)}, u32[]{:S(2)}) async-start(bf16[32,3,512]{2,1,0:T(4,128)(2,1)} %broadcast_in_dim.16), calls=%async_computation | async-start | bytes 262144 | tf_op jit(solution)/shard_map/all_to_all | solution.py:30
  47.9 0.7 copy-start.8
  47.9 0.7 copy-start.10
  78.8 5.6 %copy-start.1 = (bf16[2,512,128]{2,1,0:T(8,128)(2,1)S(1)}, bf16[2,512,128]{2,1,0:T(8,128)(2,1)}, u32[]{:S(2)}) copy-start(bf16[2,512,128]{2,1,0:T(8,128)(2,1)} %param.17) | copy-start | bytes 786436
  79.7 9.8 %all-to-all-start.2 = ((f32[8,1,96]{2,1,0:T(1,128)}), f32[8,1,96]{2,1,0:T(1,128)S(1)}, u32[]{:S(2)}, u32[]{:S(2)}) async-start(f32[8,1,96]{2,1,0:T(1,128)} %broadcast_in_dim.18), calls=%async_computation.2 | async-start | bytes 8192 | tf_op jit(solution)/shard_map/all_to_all | solution.py:30
  84.3 0.9 copy-start.2
  85.3 0.9 copy-start.4
  85.3 1.1 copy-start.5
  85.3 1.3 copy-start.6
  86.2 13.1 %copy-start = (f32[2,12,1,64,128]{4,3,2,1,0:T(8,128)S(1)}, f32[2,12,1,64,128]{4,3,2,1,0:T(8,128)}, u32[]{:S(2)}) copy-start(f32[2,12,1,64,128]{4,3,2,1,0:T(8,128)} %param.21) | copy-start | bytes 2359300
  89.5 9.5 %all-to-all-start.1 = ((bf16[8,12,448]{2,1,0:T(8,128)(2,1)}), bf16[8,12,448]{2,1,0:T(8,128)(2,1)S(1)}, u32[]{:S(2)}, u32[]{:S(2)}) async-start(bf16[8,12,448]{2,1,0:T(8,128)(2,1)} %concatenate.10), calls=%async_computation.1 | async-start | bytes 262144 | tf_op jit(solution)/shard_map/all_to_all | solution.py:24
  99.2 8.5 %copy-start.3 = (bf16[2,128,512]{2,1,0:T(8,128)(2,1)S(1)}, bf16[2,128,512]{2,1,0:T(8,128)(2,1)}, u32[]{:S(2)}) copy-start(bf16[2,128,512]{2,1,0:T(8,128)(2,1)} %param.19) | copy-start | bytes 786436
  142.9 0.7 copy-start.7
  178.6 8.5 %all-to-all-start.7 = ((f32[8,1,96]{2,1,0:T(1,128)}), f32[8,1,96]{2,1,0:T(1,128)S(1)}, u32[]{:S(2)}, u32[]{:S(2)}) async-start(f32[8,1,96]{2,1,0:T(1,128)} %broadcast_in_dim.22), calls=%async_computation.7 | async-start | bytes 8192 | tf_op jit(solution)/shard_map/all_to_all | solution.py:30
  187.1 9.5 %all-to-all-start.6 = ((bf16[8,12,448]{2,1,0:T(8,128)(2,1)}), bf16[8,12,448]{2,1,0:T(8,128)(2,1)S(1)}, u32[]{:S(2)}, u32[]{:S(2)}) async-start(bf16[8,12,448]{2,1,0:T(8,128)(2,1)} %concatenate.11), calls=%async_computation.6 | async-start | bytes 262144 | tf_op jit(solution)/shard_map/all_to_all | solution.py:24
  206.2 35.8 %all-to-all-start.9 = ((bf16[32,3,512]{2,1,0:T(4,128)(2,1)}), bf16[32,3,512]{2,1,0:T(4,128)(2,1)S(1)}, u32[]{:S(2)}, u32[]{:S(2)}) async-start(bf16[32,3,512]{2,1,0:T(4,128)(2,1)} %reshape.297), calls=%async_computation.9 | async-start | bytes 262144 | tf_op jit(solution)/shard_map/all_to_all | solution.py:24
where the time goes:
time: 244 us; the launch traced here: 243 us
  blocking collectives  83.9 us (34%)
  waiting for transfers between devices  77.4 us (32%)
  starting transfers between devices  65.9 us (27%)
  local copies, waits for them, and re-layouts  8.26 us (3%)
  other arithmetic  4.26 us (2%)
    all_to_all x3, starting transfers between devices, copy_for_each(): lax.all_to_all(jnp.broadcast_to(value[None], (length, *value.shape)), axi...  54 us
    all_to_all x3, blocking collectives, copy_for_each(): lax.all_to_all(jnp.broadcast_to(value[None], (length, *value.shape)), axi...  49 us
    all_to_all x3, waiting for transfers between devices, summed_on_arrival(): lax.all_to_all(blocks, axis, split_axis=0, concat_axis=0, tiled=True)  41.1 us
    all_to_all x3, waiting for transfers between devices, copy_for_each(): lax.all_to_all(jnp.broadcast_to(value[None], (length, *value.shape)), axi...  36.2 us
    all_to_all x1, blocking collectives, summed_on_arrival(): lax.all_to_all(blocks, axis, split_axis=0, concat_axis=0, tiled=True)  34.9 us
    all_to_all x3, starting transfers between devices, summed_on_arrival(): lax.all_to_all(blocks, axis, split_axis=0, concat_axis=0, tiled=True)  11.9 us
  transfers between devices with their start and end apart: 6, of which 6 were waited for; matrix products, arithmetic and copies ran while one was open for 2% of the time, Pallas kernels for 0%

commit v1 on v0

v1 whole, which is shorter than its diff:
```python
import jax
import jax.numpy as jnp
from jax import lax
from jax.sharding import Mesh, PartitionSpec as P

D = 4096
HEAD_KEY = 64
VALUE_CHANNELS = 128
LAYERS = 2
LANES = 128
NEAR = 4


epsilon = 1e-06
softness_factor = 16.0

TP = ("far", "near")


def size_of(axes):
    return lax.psum(1, axes)


def exchange(blocks, axes):
    return lax.all_to_all(blocks, axes, split_axis=0, concat_axis=0, tiled=True)


def copies(value, axes):
    return exchange(jnp.broadcast_to(value[None], (size_of(axes), *value.shape)), axes)


def summed(blocks):
    return blocks.astype(jnp.float32).sum(axis=0)


def two_terms(value):
    high = lax.reduce_precision(value, 8, 7)
    return high.astype(jnp.bfloat16), (value - high).astype(jnp.bfloat16)


def per_device(
    hidden_in,
    input_norm_gain,
    w_query,
    w_key,
    w_decay,
    w_value,
    w_gate,
    out_gain,
    w_out,
    decay_offset,
    state,
):
    seq_rows = state.shape[1]
    local_heads = state.shape[2]
    key_cols = local_heads * HEAD_KEY
    value_cols = local_heads * VALUE_CHANNELS
    own_rows, features = hidden_in.shape
    n_dp = size_of("dp")
    n_near = size_of("near")
    hidden = copies(hidden_in, TP).reshape(-1, features)
    own_hidden = hidden_in
    batch = hidden.shape[0]
    states = []
    for index_of_block in range(LAYERS):
        widened = hidden.astype(jnp.float32)
        squares = jnp.sum(widened * widened, axis=1, keepdims=True)
        scaled = (widened * input_norm_gain[index_of_block][None, :]).astype(jnp.bfloat16)
        partial_value = [
            jnp.dot(scaled, matrix[index_of_block], preferred_element_type=jnp.float32).astype(
                jnp.bfloat16
            )
            for matrix in (w_value, w_gate, w_query, w_key, w_decay)
        ]
        used = 2 * value_cols + 3 * key_cols
        spare = -(used + 2) % LANES
        sent = jnp.concatenate(
            [*partial_value, *two_terms(squares), jnp.zeros((batch, spare), jnp.bfloat16)], axis=1
        )
        summed_parts = summed(exchange(sent.reshape(n_dp, seq_rows, -1), "dp"))
        own_squares = jnp.sum(summed_parts[:, used : used + 2], axis=1, keepdims=True)
        inverse = lax.rsqrt(own_squares / D + epsilon)
        projected = summed_parts[:, :used] * inverse
        value_rows = projected[:, :value_cols].reshape(seq_rows, local_heads, VALUE_CHANNELS)
        gate_rows = projected[:, value_cols : 2 * value_cols].reshape(
            seq_rows, local_heads, VALUE_CHANNELS
        )
        rest = projected[:, 2 * value_cols :]
        query_rows = rest[:, :key_cols].reshape(seq_rows, local_heads, HEAD_KEY)
        key_rows = rest[:, key_cols : 2 * key_cols].reshape(
            seq_rows, local_heads, HEAD_KEY
        ) * HEAD_KEY ** (-0.5)
        decay_logits = rest[:, 2 * key_cols :]
        decay_logarithm = (
            jax.nn.log_sigmoid(decay_logits) / softness_factor + decay_offset[index_of_block]
        )
        decay_rate = jnp.exp(decay_logarithm).reshape(seq_rows, local_heads, HEAD_KEY)
        fresh = (
            decay_rate[:, :, :, None] * state[index_of_block]
            + key_rows[:, :, :, None] * value_rows[:, :, None, :]
        )
        states.append(fresh)
        readout = jnp.sum(query_rows[:, :, :, None] * fresh, axis=2)
        normed = readout * lax.rsqrt(jnp.mean(readout * readout, axis=2, keepdims=True) + epsilon)
        normed = normed * out_gain[index_of_block].reshape(local_heads, VALUE_CHANNELS)[None]
        gated_out = (
            (normed * jax.nn.silu(gate_rows)).reshape(seq_rows, value_cols).astype(jnp.bfloat16)
        )
        head_terms = jnp.dot(
            copies(gated_out, "dp").reshape(batch, value_cols),
            w_out[index_of_block],
            preferred_element_type=jnp.float32,
        ).astype(jnp.bfloat16)
        if index_of_block + 1 == LAYERS:
            own_part = summed(exchange(head_terms.reshape(-1, own_rows, features), TP))
            own_hidden = (own_hidden.astype(jnp.float32) + own_part).astype(jnp.bfloat16)
        else:
            near_sum = summed(exchange(head_terms.reshape(n_near, -1, features), "near"))
            far_sum = summed(copies(near_sum.astype(jnp.bfloat16), "far"))
            before = lax.dynamic_index_in_dim(
                hidden.reshape(n_near, -1, features), lax.axis_index("near"), 0, keepdims=False
            )
            after = (before.astype(jnp.float32) + far_sum).astype(jnp.bfloat16)
            hidden = copies(after, "near").reshape(batch, features)
            own_hidden = lax.dynamic_index_in_dim(
                hidden.reshape(-1, own_rows, features), lax.axis_index(TP), 0, keepdims=False
            )
    return (own_hidden, jnp.stack(states))


def solution(mesh):
    sizes = mesh.shape
    fine = Mesh(
        mesh.devices.reshape(sizes["grp"], sizes["tp"] // NEAR, NEAR, sizes["dp"]),
        ("grp", *TP, "dp"),
    )
    return jax.shard_map(
        per_device,
        mesh=fine,
        in_specs=(
            P(("grp", *TP), "dp"),
            P(None, "dp"),
            P(None, "dp", TP),
            P(None, "dp", TP),
            P(None, "dp", TP),
            P(None, "dp", TP),
            P(None, "dp", TP),
            P(None, TP),
            P(None, TP, "dp"),
            P(None, ("grp", "dp"), TP),
            P(None, ("grp", "dp"), TP, None, None),
        ),
        out_specs=(P(("grp", *TP), "dp"), P(None, ("grp", "dp"), TP, None, None)),
        check_vma=False,
    )
```

time: 244 us -> 216 us (0.89)
  blocking collectives: 83.9 us -> 44.3 us
  waiting for transfers between devices: 77.4 us -> 96.5 us
  starting transfers between devices: 65.9 us -> 60.3 us
    all_to_all x4 -> x5, blocking collectives: 83.9 us -> 44.3 us  [exchange(): return lax.all_to_all(blocks, axes, split_axis=0, concat_axis=0, tiled=True)]
    all_to_all x6 -> x4, waiting for transfers between devices: 77.4 us -> 96.5 us  [exchange(): return lax.all_to_all(blocks, axes, split_axis=0, concat_axis=0, tiled=True)]
    all_to_all x6 -> x4, starting transfers between devices: 65.9 us -> 60.3 us  [exchange(): return lax.all_to_all(blocks, axes, split_axis=0, concat_axis=0, tiled=True)]
  transfers between devices with their start and end apart: 6 -> 4, of which waited for: 6 -> 4; matrix products, arithmetic and copies ran while one was open for 2% -> 1% of each run, Pallas kernels for 0% -> 0%
where the time goes in v1:
time: 216 us
  waiting for transfers between devices  96.5 us (45%)
  starting transfers between devices  60.3 us (28%)
  blocking collectives  44.3 us (21%)
  local copies, waits for them, and re-layouts  7.34 us (3%)
  other arithmetic  4.35 us (2%)
    all_to_all x4, waiting for transfers between devices, exchange(): return lax.all_to_all(blocks, axes, split_axis=0, concat_axis=0, tiled=True)  96.5 us
    all_to_all x4, starting transfers between devices, exchange(): return lax.all_to_all(blocks, axes, split_axis=0, concat_axis=0, tiled=True)  60.3 us
    all_to_all x5, blocking collectives, exchange(): return lax.all_to_all(blocks, axes, split_axis=0, concat_axis=0, tiled=True)  44.3 us
  transfers between devices with their start and end apart: 4, of which 4 were waited for; matrix products, arithmetic and copies ran while one was open for 1% of the time, Pallas kernels for 0%

profile of v1, /device:TPU:40, one launch (start us, length us, event | category | flops | bytes accessed | tf_op | source)
XLA Modules:
  0.0 215.7 jit_solution(2116659769371066459)
XLA Ops:
  0.6 1.4 broadcast_in_dim.12
  2.0 45.9 %all-to-all-start = ((bf16[32,3,512]{2,1,0:T(4,128)(2,1)}), bf16[32,3,512]{2,1,0:T(4,128)(2,1)S(1)}, u32[]{:S(2)}, u32[]{:S(2)}) async-start(bf16[32,3,512]{2,1,0:T(4,128)(2,1)} %broadcast_in_dim.12), calls=%async_computation | async-start | bytes 262144 | tf_op jit(solution)/shard_map/all_to_all | solution.py:25
  48.0 30.9 %all-to-all-done = bf16[32,3,512]{2,1,0:T(4,128)(2,1)S(1)} async-done(((bf16[32,3,512]{2,1,0:T(4,128)(2,1)}), bf16[32,3,512]{2,1,0:T(4,128)(2,1)S(1)}, u32[]{:S(2)}, u32[]{:S(2)}) %all-to-all-start) | async-done | bytes 98336 | tf_op jit(solution)/shard_map/all_to_all | solution.py:25
  78.8 0.2 fusion.7
  79.5 0.7 copy-done.4
  80.4 0.6 copy-done.5
  81.7 0.3 copy-done.1
  82.0 0.2 convolution_convert_fusion.4
  82.3 0.2 convolution_convert_fusion.5
  82.5 0.8 concatenate.36
  83.3 4.7 %all-to-all-start.1 = ((bf16[8,12,512]{2,1,0:T(8,128)(2,1)}), bf16[8,12,512]{2,1,0:T(8,128)(2,1)S(1)}, u32[]{:S(2)}, u32[]{:S(2)}) async-start(bf16[8,12,512]{2,1,0:T(8,128)(2,1)} %concatenate.36), calls=%async_computation.1 | async-start | bytes 262144 | tf_op jit(solution)/shard_map/all_to_all | solution.py:25
  88.1 6.1 %all-to-all-done.1 = bf16[8,12,512]{2,1,0:T(8,128)(2,1)S(1)} async-done(((bf16[8,12,512]{2,1,0:T(8,128)(2,1)}), bf16[8,12,512]{2,1,0:T(8,128)(2,1)S(1)}, u32[]{:S(2)}, u32[]{:S(2)}) %all-to-all-start.1) | async-done | bytes 98336 | tf_op jit(solution)/shard_map/all_to_all | solution.py:25
  94.2 0.2 slice_reduce_fusion.1
  94.5 0.4 fusion.5
  95.2 7.9 %all_to_all.45 = bf16[8,12,128]{2,1,0:T(8,128)(2,1)S(1)} all-to-all(bf16[8,12,128]{2,1,0:T(8,128)(2,1)S(1)} %broadcast_in_dim.13), channel_id=1, replica_groups=mesh['grp'=2,'far'=8,'near'=4,'dp'=8] {'dp'}, dimensions={0} | all-to-all | bytes 49152 | tf_op jit(solution)/shard_map/all_to_all | solution.py:25
  103.2 8.3 %all_to_all.46 = bf16[4,24,512]{2,1,0:T(8,128)(2,1)S(1)} all-to-all(bf16[4,24,512]{2,1,0:T(8,128)(2,1)S(1)} %bitcast.96), channel_id=1, replica_groups=mesh['grp'=2,'far'=8,'near'=4,'dp'=8] {'near'}, dimensions={0} | all-to-all | bytes 196608 | tf_op jit(solution)/shard_map/all_to_all | solution.py:25
  111.5 0.7 broadcast_in_dim.14
  112.2 3.6 %all-to-all-start.4 = ((bf16[8,24,512]{2,1,0:T(8,128)(2,1)}), bf16[8,24,512]{2,1,0:T(8,128)(2,1)S(1)}, u32[]{:S(2)}, u32[]{:S(2)}) async-start(bf16[8,24,512]{2,1,0:T(8,128)(2,1)} %broadcast_in_dim.14), calls=%async_computation.4 | async-start | bytes 393216 | tf_op jit(solution)/shard_map/all_to_all | solution.py:25
  115.9 30.3 %all-to-all-done.4 = bf16[8,24,512]{2,1,0:T(8,128)(2,1)S(1)} async-done(((bf16[8,24,512]{2,1,0:T(8,128)(2,1)}), bf16[8,24,512]{2,1,0:T(8,128)(2,1)S(1)}, u32[]{:S(2)}, u32[]{:S(2)}) %all-to-all-start.4) | async-done | bytes 196640 | tf_op jit(solution)/shard_map/all_to_all | solution.py:25
  146.2 11.7 %all_to_all.47 = bf16[4,24,512]{2,1,0:T(8,128)(2,1)S(1)} all-to-all(bf16[4,24,512]{2,1,0:T(8,128)(2,1)S(1)} %broadcast_in_dim.16), channel_id=1, replica_groups=mesh['grp'=2,'far'=8,'near'=4,'dp'=8] {'near'}, dimensions={0} | all-to-all | bytes 196608 | tf_op jit(solution)/shard_map/all_to_all | solution.py:25
  158.5 0.2 convolution_convert_fusion.2
  158.7 0.2 convolution_convert_fusion.3
  159.8 8.6 %all_to_all.48 = bf16[8,12,512]{2,1,0:T(8,128)(2,1)S(1)} all-to-all(bf16[8,12,512]{2,1,0:T(8,128)(2,1)S(1)} %concatenate.42), channel_id=1, replica_groups=mesh['grp'=2,'far'=8,'near'=4,'dp'=8] {'dp'}, dimensions={0} | all-to-all | bytes 196608 | tf_op jit(solution)/shard_map/all_to_all | solution.py:25
  168.4 0.2 slice_reduce_fusion
  168.8 0.4 fusion.2
  169.4 7.9 %all_to_all.49 = bf16[8,12,128]{2,1,0:T(8,128)(2,1)S(1)} all-to-all(bf16[8,12,128]{2,1,0:T(8,128)(2,1)S(1)} %broadcast_in_dim.17), channel_id=1, replica_groups=mesh['grp'=2,'far'=8,'near'=4,'dp'=8] {'dp'}, dimensions={0} | all-to-all | bytes 49152 | tf_op jit(solution)/shard_map/all_to_all | solution.py:25
  177.4 0.7 reshape.356
  178.1 6.1 %all-to-all-start.8 = ((bf16[32,3,512]{2,1,0:T(4,128)(2,1)}), bf16[32,3,512]{2,1,0:T(4,128)(2,1)S(1)}, u32[]{:S(2)}, u32[]{:S(2)}) async-start(bf16[32,3,512]{2,1,0:T(4,128)(2,1)} %reshape.356), calls=%async_computation.8 | async-start | bytes 262144 | tf_op jit(solution)/shard_map/all_to_all | solution.py:25
  184.3 0.5 multiply_add_fusion.1
  184.8 0.9 pad_maximum_fusion
  185.7 29.3 %all-to-all-done.8 = bf16[32,3,512]{2,1,0:T(4,128)(2,1)S(1)} async-done(((bf16[32,3,512]{2,1,0:T(4,128)(2,1)}), bf16[32,3,512]{2,1,0:T(4,128)(2,1)S(1)}, u32[]{:S(2)}, u32[]{:S(2)}) %all-to-all-start.8) | async-done | bytes 98336 | tf_op jit(solution)/shard_map/all_to_all | solution.py:25
  215.1 0.6 fusion.44
  (83 shorter events, 4.4 us)
Async XLA Ops:
  2.0 45.9 %copy-start.8 = (f32[2,512]{1,0:T(2,128)S(1)}, f32[2,512]{1,0:T(2,128)}, u32[]{:S(2)}) copy-start(f32[2,512]{1,0:T(2,128)} %param.12) | copy-start | bytes 12292
  2.0 45.9 %copy-start.7 = (f32[2,12,64]{2,0,1:T(2,128)S(1)}, f32[2,12,64]{2,0,1:T(2,128)}, u32[]{:S(2)}) copy-start(f32[2,12,64]{2,0,1:T(2,128)} %param.20) | copy-start | bytes 18436
  2.0 76.8 %all-to-all-start = ((bf16[32,3,512]{2,1,0:T(4,128)(2,1)}), bf16[32,3,512]{2,1,0:T(4,128)(2,1)S(1)}, u32[]{:S(2)}, u32[]{:S(2)}) async-start(bf16[32,3,512]{2,1,0:T(4,128)(2,1)} %broadcast_in_dim.12), calls=%async_computation | async-start | bytes 262144 | tf_op jit(solution)/shard_map/all_to_all | solution.py:25
  79.2 0.9 copy-start.4
  80.1 0.9 copy-start.5
  80.4 0.9 copy-start.6
  81.0 1.0 copy-start.1
  81.4 1.0 copy-start.2
  82.0 12.5 %copy-start = (f32[2,12,1,64,128]{4,3,2,1,0:T(8,128)S(1)}, f32[2,12,1,64,128]{4,3,2,1,0:T(8,128)}, u32[]{:S(2)}) copy-start(f32[2,12,1,64,128]{4,3,2,1,0:T(8,128)} %param.21) | copy-start | bytes 2359300
  83.3 4.7 %copy-start.9 = (f32[2,128]{1,0:T(2,128)S(1)}, f32[2,128]{1,0:T(2,128)}, u32[]{:S(2)}) copy-start(f32[2,128]{1,0:T(2,128)} %param.18) | copy-start | bytes 3076
  83.3 10.8 %all-to-all-start.1 = ((bf16[8,12,512]{2,1,0:T(8,128)(2,1)}), bf16[8,12,512]{2,1,0:T(8,128)(2,1)S(1)}, u32[]{:S(2)}, u32[]{:S(2)}) async-start(bf16[8,12,512]{2,1,0:T(8,128)(2,1)} %concatenate.36), calls=%async_computation.1 | async-start | bytes 262144 | tf_op jit(solution)/shard_map/all_to_all | solution.py:25
  94.5 8.5 %copy-start.3 = (bf16[2,128,512]{2,1,0:T(8,128)(2,1)S(1)}, bf16[2,128,512]{2,1,0:T(8,128)(2,1)}, u32[]{:S(2)}) copy-start(bf16[2,128,512]{2,1,0:T(8,128)(2,1)} %param.19) | copy-start | bytes 786436
  112.2 34.0 %all-to-all-start.4 = ((bf16[8,24,512]{2,1,0:T(8,128)(2,1)}), bf16[8,24,512]{2,1,0:T(8,128)(2,1)S(1)}, u32[]{:S(2)}, u32[]{:S(2)}) async-start(bf16[8,24,512]{2,1,0:T(8,128)(2,1)} %broadcast_in_dim.14), calls=%async_computation.4 | async-start | bytes 393216 | tf_op jit(solution)/shard_map/all_to_all | solution.py:25
  178.1 36.9 %all-to-all-start.8 = ((bf16[32,3,512]{2,1,0:T(4,128)(2,1)}), bf16[32,3,512]{2,1,0:T(4,128)(2,1)S(1)}, u32[]{:S(2)}, u32[]{:S(2)}) async-start(bf16[32,3,512]{2,1,0:T(4,128)(2,1)} %reshape.356), calls=%async_computation.8 | async-start | bytes 262144 | tf_op jit(solution)/shard_map/all_to_all | solution.py:25

commit v2 on v1

v2 whole, which is shorter than its diff:
```python
import jax
import jax.numpy as jnp
from jax import lax
from jax.sharding import Mesh, PartitionSpec as P

D = 4096
HEAD_KEY = 64
VALUE_CHANNELS = 128
NEAR = 4
CORES = 2


epsilon = 1e-06
softness_factor = 16.0

TP = ("far", "near")
DP = ("x", "core")
LOCAL = ("near", *DP)


def size_of(axes):
    return lax.psum(1, axes)


def exchange(blocks, axes):
    return lax.all_to_all(blocks, axes, split_axis=0, concat_axis=0, tiled=True)


def copies(value, axes):
    return exchange(jnp.broadcast_to(value[None], (size_of(axes), *value.shape)), axes)


def summed(blocks):
    return blocks.astype(jnp.float32).sum(axis=0)


def dot(left, right):
    return jnp.dot(left, right, preferred_element_type=jnp.float32)


def from_ring(value):
    n = size_of("x")
    onward = [(i, (i + 1) % n) for i in range(n)]
    back = [(i, (i - 1) % n) for i in range(n)]
    half = value.shape[0] // 2
    found = {0: value}
    ahead = behind = value
    for step in range(1, n // 2 + 1):
        if 2 * step == n:
            ahead = lax.ppermute(ahead[:half], "x", onward)
            behind = lax.ppermute(behind[half:], "x", back)
            found[step] = jnp.concatenate([ahead, behind], axis=0)
        else:
            found[step] = ahead = lax.ppermute(ahead, "x", onward)
            found[n - step] = behind = lax.ppermute(behind, "x", back)
    return jnp.stack([found[i] for i in range(n)])


def from_all(value):
    ours = from_ring(value)
    return ours, lax.ppermute(ours, "core", [(0, 1), (1, 0)])


def turned(blocks):
    n, cores = size_of("x"), size_of("core")
    blocks = blocks.reshape(n, cores, *blocks.shape[1:])
    place = lax.axis_index("x")
    chips = [
        lax.dynamic_index_in_dim(blocks, lax.rem(place - s + n, n), 0, keepdims=False)
        for s in range(n)
    ]
    blocks = jnp.stack(chips, axis=1)
    return jnp.where(lax.axis_index("core") == 0, blocks, blocks[::-1])


def turned_back(blocks):
    n = size_of("x")
    place = lax.axis_index("x")
    blocks = jnp.where(lax.axis_index("core") == 0, blocks, blocks[::-1])
    chips = [
        lax.dynamic_index_in_dim(blocks, lax.rem(place - s + n, n), 1, keepdims=False)
        for s in range(n)
    ]
    blocks = jnp.stack(chips, axis=0)
    return blocks.reshape(-1, *blocks.shape[2:])


def three_terms(value):
    terms = []
    for _ in range(3):
        term = lax.reduce_precision(value, 8, 7)
        terms.append(term.astype(jnp.bfloat16))
        value = value - term
    return terms


def mixed_over_time(projected, squares, decay_offset, state, out_gain):
    seq_rows, local_heads = state.shape[:2]
    key_cols = local_heads * HEAD_KEY
    value_cols = local_heads * VALUE_CHANNELS
    projected = projected * lax.rsqrt(squares / D + epsilon)[:, None]
    value_rows = projected[:, :value_cols].reshape(seq_rows, local_heads, VALUE_CHANNELS)
    gate_rows = projected[:, value_cols : 2 * value_cols].reshape(
        seq_rows, local_heads, VALUE_CHANNELS
    )
    rest = projected[:, 2 * value_cols :]
    query_rows = rest[:, :key_cols].reshape(seq_rows, local_heads, HEAD_KEY)
    key_rows = rest[:, key_cols : 2 * key_cols].reshape(
        seq_rows, local_heads, HEAD_KEY
    ) * HEAD_KEY ** (-0.5)
    decay_logits = rest[:, 2 * key_cols : 3 * key_cols]
    decay_logarithm = jax.nn.log_sigmoid(decay_logits) / softness_factor + decay_offset
    decay_rate = jnp.exp(decay_logarithm).reshape(seq_rows, local_heads, HEAD_KEY)
    fresh = (
        decay_rate[:, :, :, None] * state + key_rows[:, :, :, None] * value_rows[:, :, None, :]
    )
    readout = jnp.sum(query_rows[:, :, :, None] * fresh, axis=2)
    normed = readout * lax.rsqrt(jnp.mean(readout * readout, axis=2, keepdims=True) + epsilon)
    normed = normed * out_gain.reshape(local_heads, VALUE_CHANNELS)[None]
    gated_out = (normed * jax.nn.silu(gate_rows)).reshape(seq_rows, value_cols)
    return gated_out.astype(jnp.bfloat16), fresh


def per_device(
    hidden_in,
    input_norm_gain,
    w_query,
    w_key,
    w_decay,
    w_value,
    w_gate,
    out_gain,
    w_out,
    decay_offset,
    state,
):
    seq_rows = state.shape[1]
    value_cols = w_out.shape[1]
    own_rows, features = hidden_in.shape
    n_dp, n_near = size_of(DP), size_of("near")
    matrices = (w_value, w_gate, w_query, w_key, w_decay)

    with jax.named_scope("gather_hidden"):
        hidden = copies(hidden_in, TP).reshape(-1, features)
    with jax.named_scope("fetch_out"):
        out_first = from_all(w_out[0])

    widened = hidden.astype(jnp.float32)
    scaled = (widened * input_norm_gain[0][None, :]).astype(jnp.bfloat16)
    partial_value = [dot(scaled, matrix[0]).astype(jnp.bfloat16) for matrix in matrices]
    used = sum(part.shape[1] for part in partial_value)
    sent = jnp.concatenate([hidden, *partial_value], axis=1)
    with jax.named_scope("sum_partials"):
        arrived = exchange(sent.reshape(n_dp, seq_rows, -1), DP)
    own = arrived[:, :, :features].astype(jnp.float32)
    gated_out, fresh_first = mixed_over_time(
        summed(arrived[:, :, features:]),
        jnp.sum(own * own, axis=(0, 2)),
        decay_offset[0],
        state[0],
        out_gain[0],
    )

    with jax.named_scope("fetch_in"):
        weights, arrived = lax.optimization_barrier(
            ([matrix[1] for matrix in matrices] + [w_out[1], input_norm_gain[1]], arrived)
        )
        rows = jnp.concatenate(
            [
                *(matrix.T for matrix in weights[:-2]),
                weights[-2],
                jnp.stack(three_terms(weights[-1])),
                jnp.zeros((13, features), jnp.bfloat16),
            ],
            axis=0,
        )
        fetched = from_all(rows)

    def out_terms(gated_out, pieces):
        return jnp.stack(
            [jnp.stack([dot(gated_out, part[i]) for i in range(part.shape[0])]) for part in pieces]
        ).astype(jnp.bfloat16)

    head_terms = turned_back(out_terms(gated_out, out_first))
    with jax.named_scope("near_sum"):
        near_sum = summed(exchange(head_terms.reshape(n_near, -1, seq_rows, features), "near"))
    with jax.named_scope("far_sum"):
        far_sum = summed(copies(near_sum.astype(jnp.bfloat16), "far"))
    before = lax.dynamic_index_in_dim(
        own.reshape(n_near, -1, seq_rows, features), lax.axis_index("near"), 0, keepdims=False
    )
    after = (before + far_sum).astype(jnp.bfloat16)
    with jax.named_scope("near_gather"):
        hidden = copies(after, "near").reshape(n_dp, seq_rows, features)

    widened = hidden.astype(jnp.float32)
    projected = 0.0
    for block, part in zip(turned(hidden), fetched):
        gain = summed(jnp.moveaxis(part[:, used + value_cols : used + value_cols + 3], 1, 0))
        scaled = (block.astype(jnp.float32) * gain[:, None, :]).astype(jnp.bfloat16)
        projected = projected + lax.dot_general(
            scaled,
            part[:, :used],
            (((0, 2), (0, 2)), ((), ())),
            preferred_element_type=jnp.float32,
        )
    gated_out, fresh_second = mixed_over_time(
        projected, jnp.sum(widened * widened, axis=(0, 2)), decay_offset[1], state[1], out_gain[1]
    )
    head_terms = turned_back(
        out_terms(gated_out, [part[:, used : used + value_cols] for part in fetched])
    )

    def to_holders(value):
        value = value.reshape(n_dp, n_near, own_rows, features)
        return jnp.moveaxis(value, 1, 0).reshape(n_near * n_dp, own_rows, features)

    with jax.named_scope("local_sum"):
        sent = jnp.concatenate(
            [to_holders(head_terms), to_holders(hidden)], axis=1
        )
        arrived = exchange(sent, LOCAL).reshape(n_near, n_dp, 2 * own_rows, features)
    before = lax.dynamic_index_in_dim(
        arrived[0], lax.axis_index("far"), 0, keepdims=False
    )[own_rows:]
    local_sum = summed(arrived[:, :, :own_rows])
    with jax.named_scope("far_scatter"):
        mixed = summed(exchange(local_sum.astype(jnp.bfloat16), "far"))
    hidden_out = (before.astype(jnp.float32) + mixed).astype(jnp.bfloat16)
    return (hidden_out, jnp.stack([fresh_first, fresh_second]))


def solution(mesh):
    sizes = mesh.shape
    fine = Mesh(
        mesh.devices.reshape(sizes["grp"], sizes["tp"] // NEAR, NEAR, sizes["dp"] // CORES, CORES),
        ("grp", *TP, *DP),
    )
    return jax.shard_map(
        per_device,
        mesh=fine,
        in_specs=(
            P(("grp", *TP), DP),
            P(None, DP),
            P(None, DP, TP),
            P(None, DP, TP),
            P(None, DP, TP),
            P(None, DP, TP),
            P(None, DP, TP),
            P(None, TP),
            P(None, TP, DP),
            P(None, ("grp", *DP), TP),
            P(None, ("grp", *DP), TP, None, None),
        ),
        out_specs=(P(("grp", *TP), DP), P(None, ("grp", *DP), TP, None, None)),
        check_vma=False,
    )
```

time: 216 us -> 228 us (1.056)
  starting transfers between devices: 60.3 us -> 108 us
  blocking collectives: 44.3 us -> 0 us
  waiting for transfers between devices: 96.5 us -> 78.7 us
  matrix products: 1.88 us -> 11.6 us
  local copies, waits for them, and re-layouts: 7.34 us -> 14.9 us
  other arithmetic: 4.35 us -> 11.9 us
    all_to_all x5 -> x0, blocking collectives: 44.3 us -> none  [exchange(): return lax.all_to_all(blocks, axes, split_axis=0, concat_axis=0, tiled=True)]
    ppermute x0 -> x10, starting transfers between devices: none -> 32.7 us  [the longest x2 9.92 us: from_ring(): behind = lax.ppermute(behind[half:], 'x', back)]
    all_to_all x4 -> x7, waiting for transfers between devices: 96.5 us -> 67.8 us  [exchange(): return lax.all_to_all(blocks, axes, split_axis=0, concat_axis=0, tiled=True)]
    all_to_all x4 -> x7, starting transfers between devices: 60.3 us -> 75.5 us  [exchange(): return lax.all_to_all(blocks, axes, split_axis=0, concat_axis=0, tiled=True)]
    ppermute x0 -> x10, waiting for transfers between devices: none -> 10.9 us  [the longest x2 5.95 us: from_ring(): found[step] = ahead = lax.ppermute(ahead, 'x', onward)]
    dot_general x12 -> x23, matrix products: 1.88 us -> 11.6 us  [the longest x21 7.45 us: dot(): return jnp.dot(left, right, preferred_element_type=jnp.float32)]
    reduce_sum x5 -> x7, other arithmetic: 0.17 us -> 4.11 us  [summed(): return blocks.astype(jnp.float32).sum(axis=0)]
    another operation x1 -> x13, other arithmetic: 0.93 us -> 4.75 us  [the longest x3 1.87 us: from_ring(): return jnp.stack([found[i] for i in range(n)])]
  transfers between devices with their start and end apart: 4 -> 17, of which waited for: 4 -> 9; matrix products, arithmetic and copies ran while one was open for 1% -> 10% of each run, Pallas kernels for 0% -> 0%
where the time goes in v2:
time: 228 us; the launch traced here: 227 us
  starting transfers between devices  108 us (47%)
  waiting for transfers between devices  78.7 us (35%)
  local copies, waits for them, and re-layouts  14.9 us (7%)
  other arithmetic  11.9 us (5%)
  matrix products  11.6 us (5%)
    all_to_all x7, starting transfers between devices, exchange(): return lax.all_to_all(blocks, axes, split_axis=0, concat_axis=0, tiled=True)  75.5 us
    all_to_all x7, waiting for transfers between devices, exchange(): return lax.all_to_all(blocks, axes, split_axis=0, concat_axis=0, tiled=True)  67.8 us
    ppermute x2, starting transfers between devices, from_ring(): behind = lax.ppermute(behind[half:], 'x', back)  9.92 us
    ppermute x2, starting transfers between devices, from_ring(): found[n - step] = behind = lax.ppermute(behind, 'x', back)  8.12 us
    dot_general x21, matrix products, dot(): return jnp.dot(left, right, preferred_element_type=jnp.float32)  7.45 us
    ppermute x2, starting transfers between devices, from_ring(): found[step] = ahead = lax.ppermute(ahead, 'x', onward)  6.11 us
    ppermute x2, waiting for transfers between devices, from_ring(): found[step] = ahead = lax.ppermute(ahead, 'x', onward)  5.95 us
  transfers between devices with their start and end apart: 17, of which 9 were waited for; matrix products, arithmetic and copies ran while one was open for 10% of the time, Pallas kernels for 0%

profile of v2, /device:TPU:40, one launch (start us, length us, event | category | flops | bytes accessed | tf_op | source)
XLA Modules:
  0.0 226.8 jit_solution(10851111048224031313)
XLA Ops:
  1.7 3.6 %collective-permute-start = (bf16[128,512]{1,0:T(8,128)(2,1)S(1)}, bf16[128,512]{1,0:T(8,128)(2,1)S(1)}, u32[]{:S(2)}, u32[]{:S(2)}) collective-permute-start(bf16[128,512]{1,0:T(8,128)(2,1)S(1)} %get-tuple-element.19), channel_id=1, source_target_pairs={{0,2},{2,4},{4,6},{6,0},{1,3},{3,5},{5,7},{7,1},{8,10},{10,12},{12... | collective-permute-start | bytes 393224 | tf_op jit(solution)/shard_map/fetch_out/ppermute | solution.py:54
  5.3 3.5 %collective-permute-start.2 = (bf16[128,512]{1,0:T(8,128)(2,1)S(1)}, bf16[128,512]{1,0:T(8,128)(2,1)S(1)}, u32[]{:S(2)}, u32[]{:S(2)}) collective-permute-start(bf16[128,512]{1,0:T(8,128)(2,1)S(1)} %get-tuple-element.19), channel_id=1, source_target_pairs={{0,6},{2,0},{4,2},{6,4},{1,7},{3,1},{5,3},{7,5},{8,14},{10,8},{12,... | collective-permute-start | bytes 393224 | tf_op jit(solution)/shard_map/fetch_out/ppermute | solution.py:55
  8.9 1.4 broadcast_in_dim.10
  10.3 45.8 %all-to-all-start = ((bf16[32,3,512]{2,1,0:T(4,128)(2,1)}), bf16[32,3,512]{2,1,0:T(4,128)(2,1)S(1)}, u32[]{:S(2)}, u32[]{:S(2)}) async-start(bf16[32,3,512]{2,1,0:T(4,128)(2,1)} %broadcast_in_dim.10), calls=%async_computation | async-start | bytes 262144 | tf_op jit(solution)/shard_map/gather_hidden/all_to_all | solution.py:26
  56.0 1.5 slice_bitcast_fusion.29
  57.5 1.4 fusion.71
  59.7 2.4 %collective-permute-start.1 = (bf16[64,512]{1,0:T(8,128)(2,1)S(1)}, bf16[64,512]{1,0:T(8,128)(2,1)S(1)}, u32[]{:S(2)}, u32[]{:S(2)}) collective-permute-start(bf16[64,512]{1,0:T(8,128)(2,1)S(1)} %slice.251), channel_id=1, source_target_pairs={{0,2},{2,4},{4,6},{6,0},{1,3},{3,5},{5,7},{7,1},{8,10},{10,12},{12... | collective-permute-start | bytes 196616 | tf_op jit(solution)/shard_map/fetch_out/ppermute | solution.py:50
  63.3 4.8 %collective-permute-start.3 = (bf16[64,512]{1,0:T(8,128)(2,1)S(1)}, bf16[64,512]{1,0:T(8,128)(2,1)S(1)}, u32[]{:S(2)}, u32[]{:S(2)}) collective-permute-start(bf16[64,512]{1,0:T(8,128)(2,1)S(1)} %slice.252), channel_id=1, source_target_pairs={{0,6},{2,0},{4,2},{6,4},{1,7},{3,1},{5,3},{7,5},{8,14},{10,8},{12,... | collective-permute-start | bytes 196616 | tf_op jit(solution)/shard_map/fetch_out/ppermute | solution.py:51
  68.1 18.3 %all-to-all-done = bf16[32,3,512]{2,1,0:T(4,128)(2,1)S(1)} async-done(((bf16[32,3,512]{2,1,0:T(4,128)(2,1)}), bf16[32,3,512]{2,1,0:T(4,128)(2,1)S(1)}, u32[]{:S(2)}, u32[]{:S(2)}) %all-to-all-start) | async-done | bytes 98336 | tf_op jit(solution)/shard_map/gather_hidden/all_to_all | solution.py:26
  89.7 3.6 %all-to-all-start.1 = ((bf16[8,12,960]{2,1,0:T(8,128)(2,1)}), bf16[8,12,960]{2,1,0:T(8,128)(2,1)S(1)}, u32[]{:S(2)}, u32[]{:S(2)}) async-start(bf16[8,12,960]{2,1,0:T(8,128)(2,1)} %concatenate.34), calls=%async_computation.1 | async-start | bytes 524288 | tf_op jit(solution)/shard_map/sum_partials/all_to_all | solution.py:26
  93.5 2.3 %collective-permute-start.4 = (bf16[4,128,512]{2,1,0:T(8,128)(2,1)S(1)}, bf16[4,128,512]{2,1,0:T(8,128)(2,1)S(1)}, u32[]{:S(2)}, u32[]{:S(2)}) collective-permute-start(bf16[4,128,512]{2,1,0:T(8,128)(2,1)S(1)} %pad_maximum_fusion.2), channel_id=1, source_target_pairs={{0,1},{1,0},{2,3},{3,2},{4,5},{5,4},{6,7},{7,6},{8,9},{9,8},{10,11... | collective-permute-start | bytes 1572872 | tf_op jit(solution)/shard_map/fetch_out/ppermute | solution.py:61
  95.8 4.9 %all-to-all-done.1 = bf16[8,12,960]{2,1,0:T(8,128)(2,1)S(1)} async-done(((bf16[8,12,960]{2,1,0:T(8,128)(2,1)}), bf16[8,12,960]{2,1,0:T(8,128)(2,1)S(1)}, u32[]{:S(2)}, u32[]{:S(2)}) %all-to-all-start.1) | async-done | bytes 184352 | tf_op jit(solution)/shard_map/sum_partials/all_to_all | solution.py:26
  103.8 3.4 %all-to-all-start.2 = ((bf16[4,2,12,512]{3,1,2,0:T(2,128)(2,1)}), bf16[4,2,12,512]{3,1,2,0:T(2,128)(2,1)S(1)}, u32[]{:S(2)}, u32[]{:S(2)}) async-start(bf16[4,2,12,512]{3,1,2,0:T(2,128)(2,1)} %pad_maximum_fusion.7), calls=%async_computation.2 | async-start | bytes 196608 | tf_op jit(solution)/shard_map/near_sum/all_to_all | solution.py:26
  108.6 2.5 %collective-permute-start.5 = (bf16[592,512]{1,0:T(8,128)(2,1)S(1)}, bf16[592,512]{1,0:T(8,128)(2,1)S(1)}, u32[]{:S(2)}, u32[]{:S(2)}) collective-permute-start(bf16[592,512]{1,0:T(8,128)(2,1)S(1)} %concatenate.36), channel_id=1, source_target_pairs={{0,2},{2,4},{4,6},{6,0},{1,3},{3,5},{5,7},{7,1},{8,10},{10,12},{12... | collective-permute-start | bytes 1818632 | tf_op jit(solution)/shard_map/fetch_in/ppermute | solution.py:54
  111.1 4.6 %collective-permute-start.7 = (bf16[592,512]{1,0:T(8,128)(2,1)S(1)}, bf16[592,512]{1,0:T(8,128)(2,1)S(1)}, u32[]{:S(2)}, u32[]{:S(2)}) collective-permute-start(bf16[592,512]{1,0:T(8,128)(2,1)S(1)} %concatenate.36), channel_id=1, source_target_pairs={{0,6},{2,0},{4,2},{6,4},{1,7},{3,1},{5,3},{7,5},{8,14},{10,8},{12,... | collective-permute-start | bytes 1818632 | tf_op jit(solution)/shard_map/fetch_in/ppermute | solution.py:55
  116.6 4.2 %all-to-all-start.3 = ((bf16[8,2,12,512]{3,1,2,0:T(2,128)(2,1)}), bf16[8,2,12,512]{3,1,2,0:T(2,128)(2,1)}, u32[]{:S(2)}, u32[]{:S(2)}) async-start(bf16[8,2,12,512]{3,1,2,0:T(2,128)(2,1)} %broadcast_in_dim.11), calls=%async_computation.3 | async-start | bytes 393216 | tf_op jit(solution)/shard_map/far_sum/all_to_all | solution.py:26
  120.8 6.0 %collective-permute-done.5 = bf16[592,512]{1,0:T(8,128)(2,1)S(1)} collective-permute-done((bf16[592,512]{1,0:T(8,128)(2,1)S(1)}, bf16[592,512]{1,0:T(8,128)(2,1)S(1)}, u32[]{:S(2)}, u32[]{:S(2)}) %collective-permute-start.5) | collective-permute-done | bytes 606240 | tf_op jit(solution)/shard_map/fetch_in/ppermute | solution.py:54
  126.8 2.0 collective-permute-start.6
  128.8 5.2 %collective-permute-start.8 = (bf16[296,512]{1,0:T(8,128)(2,1)S(1)}, bf16[296,512]{1,0:T(8,128)(2,1)S(1)}, u32[]{:S(2)}, u32[]{:S(2)}) collective-permute-start(bf16[296,512]{1,0:T(8,128)(2,1)S(1)} %slice.258), channel_id=1, source_target_pairs={{0,6},{2,0},{4,2},{6,4},{1,7},{3,1},{5,3},{7,5},{8,14},{10,8},{12,... | collective-permute-start | bytes 909320 | tf_op jit(solution)/shard_map/fetch_in/ppermute | solution.py:51
  134.0 3.7 %collective-permute-done.6 = bf16[296,512]{1,0:T(8,128)(2,1)S(1)} collective-permute-done((bf16[296,512]{1,0:T(8,128)(2,1)S(1)}, bf16[296,512]{1,0:T(8,128)(2,1)S(1)}, u32[]{:S(2)}, u32[]{:S(2)}) %collective-permute-start.6) | collective-permute-done | bytes 303136 | tf_op jit(solution)/shard_map/fetch_in/ppermute | solution.py:50
  138.9 1.8 pad_maximum_fusion
  140.7 1.9 collective-permute-start.9
  142.7 8.9 %all-to-all-done.3 = bf16[8,2,12,512]{3,1,2,0:T(2,128)(2,1)} async-done(((bf16[8,2,12,512]{3,1,2,0:T(2,128)(2,1)}), bf16[8,2,12,512]{3,1,2,0:T(2,128)(2,1)}, u32[]{:S(2)}, u32[]{:S(2)}) %all-to-all-start.3) | async-done | bytes 196640 | tf_op jit(solution)/shard_map/far_sum/all_to_all | solution.py:26
  153.4 6.6 %all-to-all-start.4 = ((bf16[4,2,12,512]{3,1,2,0:T(2,128)(2,1)}), bf16[4,2,12,512]{3,1,2,0:T(2,128)(2,1)S(1)}, u32[]{:S(2)}, u32[]{:S(2)}) async-start(bf16[4,2,12,512]{3,1,2,0:T(2,128)(2,1)} %broadcast_in_dim.13), calls=%async_computation.4 | async-start | bytes 196608 | tf_op jit(solution)/shard_map/near_gather/all_to_all | solution.py:26
  160.0 1.4 convert_reduce_fusion.4
  161.4 4.5 %all-to-all-done.4 = bf16[4,2,12,512]{3,1,2,0:T(2,128)(2,1)S(1)} async-done(((bf16[4,2,12,512]{3,1,2,0:T(2,128)(2,1)}), bf16[4,2,12,512]{3,1,2,0:T(2,128)(2,1)S(1)}, u32[]{:S(2)}, u32[]{:S(2)}) %all-to-all-start.4) | async-done | bytes 98336 | tf_op jit(solution)/shard_map/near_gather/all_to_all | solution.py:26
  169.8 2.1 fusion.7
  171.9 2.1 fusion.13
  180.8 4.8 %all-to-all-start.5 = ((bf16[32,6,512]{2,1,0:T(8,128)(2,1)}), bf16[32,6,512]{2,1,0:T(8,128)(2,1)S(1)}, u32[]{:S(2)}, u32[]{:S(2)}) async-start(bf16[32,6,512]{2,1,0:T(8,128)(2,1)} %copy.151), calls=%async_computation.5 | async-start | bytes 524288 | tf_op jit(solution)/shard_map/local_sum/all_to_all | solution.py:26
  185.6 10.1 %all-to-all-done.5 = bf16[32,6,512]{2,1,0:T(8,128)(2,1)S(1)} async-done(((bf16[32,6,512]{2,1,0:T(8,128)(2,1)}), bf16[32,6,512]{2,1,0:T(8,128)(2,1)S(1)}, u32[]{:S(2)}, u32[]{:S(2)}) %all-to-all-start.5) | async-done | bytes 196640 | tf_op jit(solution)/shard_map/local_sum/all_to_all | solution.py:26
  196.4 7.1 %all-to-all-start.6 = ((bf16[8,3,512]{2,1,0:T(4,128)(2,1)}), bf16[8,3,512]{2,1,0:T(4,128)(2,1)S(1)}, u32[]{:S(2)}, u32[]{:S(2)}) async-start(bf16[8,3,512]{2,1,0:T(4,128)(2,1)} %slice_reduce_fusion), calls=%async_computation.6 | async-start | bytes 65536 | tf_op jit(solution)/shard_map/far_scatter/all_to_all | solution.py:26
  205.0 21.2 %all-to-all-done.6 = bf16[8,3,512]{2,1,0:T(4,128)(2,1)S(1)} async-done(((bf16[8,3,512]{2,1,0:T(4,128)(2,1)}), bf16[8,3,512]{2,1,0:T(4,128)(2,1)S(1)}, u32[]{:S(2)}, u32[]{:S(2)}) %all-to-all-start.6) | async-done | bytes 24608 | tf_op jit(solution)/shard_map/far_scatter/all_to_all | solution.py:26
  (155 shorter events, 28.2 us)
Async XLA Ops:
  0.6 87.1 %copy-start.6 = (bf16[2,512,64]{1,2,0:T(8,128)(2,1)S(1)}, bf16[2,512,64]{1,2,0:T(8,128)(2,1)}, u32[]{:S(2)}) copy-start(bf16[2,512,64]{1,2,0:T(8,128)(2,1)} %param.15) | copy-start | bytes 393220
  0.6 87.2 %copy-start.3 = (bf16[2,512,128]{2,1,0:T(8,128)(2,1)S(1)}, bf16[2,512,128]{2,1,0:T(8,128)(2,1)}, u32[]{:S(2)}) copy-start(bf16[2,512,128]{2,1,0:T(8,128)(2,1)} %param.16) | copy-start | bytes 786436
  0.7 87.4 %copy-start.2 = (bf16[2,512,128]{2,1,0:T(8,128)(2,1)S(1)}, bf16[2,512,128]{2,1,0:T(8,128)(2,1)}, u32[]{:S(2)}) copy-start(bf16[2,512,128]{2,1,0:T(8,128)(2,1)} %param.17) | copy-start | bytes 786436
  0.7 87.6 %copy-start.4 = (bf16[2,512,64]{1,2,0:T(8,128)(2,1)S(1)}, bf16[2,512,64]{1,2,0:T(8,128)(2,1)}, u32[]{:S(2)}) copy-start(bf16[2,512,64]{1,2,0:T(8,128)(2,1)} %param.13) | copy-start | bytes 393220
  1.7 57.9 %collective-permute-start = (bf16[128,512]{1,0:T(8,128)(2,1)S(1)}, bf16[128,512]{1,0:T(8,128)(2,1)S(1)}, u32[]{:S(2)}, u32[]{:S(2)}) collective-permute-start(bf16[128,512]{1,0:T(8,128)(2,1)S(1)} %get-tuple-element.19), channel_id=1, source_target_pairs={{0,2},{2,4},{4,6},{6,0},{1,3},{3,5},{5,7},{7,1},{8,10},{10,12},{12... | collective-permute-start | bytes 393224 | tf_op jit(solution)/shard_map/fetch_out/ppermute | solution.py:54
  5.3 58.0 %collective-permute-start.2 = (bf16[128,512]{1,0:T(8,128)(2,1)S(1)}, bf16[128,512]{1,0:T(8,128)(2,1)S(1)}, u32[]{:S(2)}, u32[]{:S(2)}) collective-permute-start(bf16[128,512]{1,0:T(8,128)(2,1)S(1)} %get-tuple-element.19), channel_id=1, source_target_pairs={{0,6},{2,0},{4,2},{6,4},{1,7},{3,1},{5,3},{7,5},{8,14},{10,8},{12,... | collective-permute-start | bytes 393224 | tf_op jit(solution)/shard_map/fetch_out/ppermute | solution.py:55
  10.3 76.2 %all-to-all-start = ((bf16[32,3,512]{2,1,0:T(4,128)(2,1)}), bf16[32,3,512]{2,1,0:T(4,128)(2,1)S(1)}, u32[]{:S(2)}, u32[]{:S(2)}) async-start(bf16[32,3,512]{2,1,0:T(4,128)(2,1)} %broadcast_in_dim.10), calls=%async_computation | async-start | bytes 262144 | tf_op jit(solution)/shard_map/gather_hidden/all_to_all | solution.py:26
  59.7 8.4 %collective-permute-start.1 = (bf16[64,512]{1,0:T(8,128)(2,1)S(1)}, bf16[64,512]{1,0:T(8,128)(2,1)S(1)}, u32[]{:S(2)}, u32[]{:S(2)}) collective-permute-start(bf16[64,512]{1,0:T(8,128)(2,1)S(1)} %slice.251), channel_id=1, source_target_pairs={{0,2},{2,4},{4,6},{6,0},{1,3},{3,5},{5,7},{7,1},{8,10},{10,12},{12... | collective-permute-start | bytes 196616 | tf_op jit(solution)/shard_map/fetch_out/ppermute | solution.py:50
  63.3 30.0 %collective-permute-start.3 = (bf16[64,512]{1,0:T(8,128)(2,1)S(1)}, bf16[64,512]{1,0:T(8,128)(2,1)S(1)}, u32[]{:S(2)}, u32[]{:S(2)}) collective-permute-start(bf16[64,512]{1,0:T(8,128)(2,1)S(1)} %slice.252), channel_id=1, source_target_pairs={{0,6},{2,0},{4,2},{6,4},{1,7},{3,1},{5,3},{7,5},{8,14},{10,8},{12,... | collective-permute-start | bytes 196616 | tf_op jit(solution)/shard_map/fetch_out/ppermute | solution.py:51
  86.5 14.5 %copy-start = (f32[2,12,1,64,128]{4,3,2,1,0:T(8,128)S(1)}, f32[2,12,1,64,128]{4,3,2,1,0:T(8,128)}, u32[]{:S(2)}) copy-start(f32[2,12,1,64,128]{4,3,2,1,0:T(8,128)} %param.21) | copy-start | bytes 2359300
  87.7 14.0 %copy-start.1 = (bf16[2,128,512]{2,1,0:T(8,128)(2,1)S(1)}, bf16[2,128,512]{2,1,0:T(8,128)(2,1)}, u32[]{:S(2)}) copy-start(bf16[2,128,512]{2,1,0:T(8,128)(2,1)} %param.19) | copy-start | bytes 786436
  89.7 10.9 %all-to-all-start.1 = ((bf16[8,12,960]{2,1,0:T(8,128)(2,1)}), bf16[8,12,960]{2,1,0:T(8,128)(2,1)S(1)}, u32[]{:S(2)}, u32[]{:S(2)}) async-start(bf16[8,12,960]{2,1,0:T(8,128)(2,1)} %concatenate.34), calls=%async_computation.1 | async-start | bytes 524288 | tf_op jit(solution)/shard_map/sum_partials/all_to_all | solution.py:26
  93.4 13.8 %copy-start.5 = (bf16[2,512,64]{1,2,0:T(8,128)(2,1)S(1)}, bf16[2,512,64]{1,2,0:T(8,128)(2,1)}, u32[]{:S(2)}) copy-start(bf16[2,512,64]{1,2,0:T(8,128)(2,1)} %param.13) | copy-start | bytes 393220
  93.5 13.7 %slice-start.1 = ((bf16[2,512,128]{2,1,0:T(8,128)(2,1)}), bf16[1,512,128]{2,1,0:T(8,128)(2,1)S(1)}, s32[]{:S(2)}) async-start(bf16[2,512,128]{2,1,0:T(8,128)(2,1)} %param.16), calls=%async_computation.8 | async-start | bytes 262144 | tf_op jit(solution)/shard_map/fetch_in/slice | solution.py:166
  93.5 13.8 %slice-start = ((bf16[2,512,128]{2,1,0:T(8,128)(2,1)}), bf16[1,512,128]{2,1,0:T(8,128)(2,1)S(1)}, s32[]{:S(2)}) async-start(bf16[2,512,128]{2,1,0:T(8,128)(2,1)} %param.17), calls=%async_computation.7 | async-start | bytes 262144 | tf_op jit(solution)/shard_map/fetch_in/slice | solution.py:166
  93.5 8.7 %collective-permute-start.4 = (bf16[4,128,512]{2,1,0:T(8,128)(2,1)S(1)}, bf16[4,128,512]{2,1,0:T(8,128)(2,1)S(1)}, u32[]{:S(2)}, u32[]{:S(2)}) collective-permute-start(bf16[4,128,512]{2,1,0:T(8,128)(2,1)S(1)} %pad_maximum_fusion.2), channel_id=1, source_target_pairs={{0,1},{1,0},{2,3},{3,2},{4,5},{5,4},{6,7},{7,6},{8,9},{9,8},{10,11... | collective-permute-start | bytes 1572872 | tf_op jit(solution)/shard_map/fetch_out/ppermute | solution.py:61
  100.9 1.1 copy-start.7
  103.8 11.9 %all-to-all-start.2 = ((bf16[4,2,12,512]{3,1,2,0:T(2,128)(2,1)}), bf16[4,2,12,512]{3,1,2,0:T(2,128)(2,1)S(1)}, u32[]{:S(2)}, u32[]{:S(2)}) async-start(bf16[4,2,12,512]{3,1,2,0:T(2,128)(2,1)} %pad_maximum_fusion.7), calls=%async_computation.2 | async-start | bytes 196608 | tf_op jit(solution)/shard_map/near_sum/all_to_all | solution.py:26
  108.6 18.2 %collective-permute-start.5 = (bf16[592,512]{1,0:T(8,128)(2,1)S(1)}, bf16[592,512]{1,0:T(8,128)(2,1)S(1)}, u32[]{:S(2)}, u32[]{:S(2)}) collective-permute-start(bf16[592,512]{1,0:T(8,128)(2,1)S(1)} %concatenate.36), channel_id=1, source_target_pairs={{0,2},{2,4},{4,6},{6,0},{1,3},{3,5},{5,7},{7,1},{8,10},{10,12},{12... | collective-permute-start | bytes 1818632 | tf_op jit(solution)/shard_map/fetch_in/ppermute | solution.py:54
  111.1 17.6 %collective-permute-start.7 = (bf16[592,512]{1,0:T(8,128)(2,1)S(1)}, bf16[592,512]{1,0:T(8,128)(2,1)S(1)}, u32[]{:S(2)}, u32[]{:S(2)}) collective-permute-start(bf16[592,512]{1,0:T(8,128)(2,1)S(1)} %concatenate.36), channel_id=1, source_target_pairs={{0,6},{2,0},{4,2},{6,4},{1,7},{3,1},{5,3},{7,5},{8,14},{10,8},{12,... | collective-permute-start | bytes 1818632 | tf_op jit(solution)/shard_map/fetch_in/ppermute | solution.py:55
  116.6 34.9 %all-to-all-start.3 = ((bf16[8,2,12,512]{3,1,2,0:T(2,128)(2,1)}), bf16[8,2,12,512]{3,1,2,0:T(2,128)(2,1)}, u32[]{:S(2)}, u32[]{:S(2)}) async-start(bf16[8,2,12,512]{3,1,2,0:T(2,128)(2,1)} %broadcast_in_dim.11), calls=%async_computation.3 | async-start | bytes 393216 | tf_op jit(solution)/shard_map/far_sum/all_to_all | solution.py:26
  126.8 10.8 %collective-permute-start.6 = (bf16[296,512]{1,0:T(8,128)(2,1)S(1)}, bf16[296,512]{1,0:T(8,128)(2,1)S(1)}, u32[]{:S(2)}, u32[]{:S(2)}) collective-permute-start(bf16[296,512]{1,0:T(8,128)(2,1)S(1)} %slice.257), channel_id=1, source_target_pairs={{0,2},{2,4},{4,6},{6,0},{1,3},{3,5},{5,7},{7,1},{8,10},{10,12},{12... | collective-permute-start | bytes 909320 | tf_op jit(solution)/shard_map/fetch_in/ppermute | solution.py:50
  128.8 10.1 %collective-permute-start.8 = (bf16[296,512]{1,0:T(8,128)(2,1)S(1)}, bf16[296,512]{1,0:T(8,128)(2,1)S(1)}, u32[]{:S(2)}, u32[]{:S(2)}) collective-permute-start(bf16[296,512]{1,0:T(8,128)(2,1)S(1)} %slice.258), channel_id=1, source_target_pairs={{0,6},{2,0},{4,2},{6,4},{1,7},{3,1},{5,3},{7,5},{8,14},{10,8},{12,... | collective-permute-start | bytes 909320 | tf_op jit(solution)/shard_map/fetch_in/ppermute | solution.py:51
  140.7 28.3 %collective-permute-start.9 = (bf16[4,592,512]{2,1,0:T(8,128)(2,1)}, bf16[4,592,512]{2,1,0:T(8,128)(2,1)}, u32[]{:S(2)}, u32[]{:S(2)}) collective-permute-start(bf16[4,592,512]{2,1,0:T(8,128)(2,1)} %pad_maximum_fusion), channel_id=1, source_target_pairs={{0,1},{1,0},{2,3},{3,2},{4,5},{5,4},{6,7},{7,6},{8,9},{9,8},{10,11... | collective-permute-start | bytes 7274504 | tf_op jit(solution)/shard_map/fetch_in/ppermute | solution.py:61
  153.4 12.4 %all-to-all-start.4 = ((bf16[4,2,12,512]{3,1,2,0:T(2,128)(2,1)}), bf16[4,2,12,512]{3,1,2,0:T(2,128)(2,1)S(1)}, u32[]{:S(2)}, u32[]{:S(2)}) async-start(bf16[4,2,12,512]{3,1,2,0:T(2,128)(2,1)} %broadcast_in_dim.13), calls=%async_computation.4 | async-start | bytes 196608 | tf_op jit(solution)/shard_map/near_gather/all_to_all | solution.py:26
  167.9 4.0 %copy-start.10 = (f32[4,512]{1,0:T(4,128)S(1)}, f32[4,512]{1,0:T(4,128)}, u32[]{:S(2)}) copy-start(f32[4,512]{1,0:T(4,128)} %convert_reduce_fusion.4) | copy-start | bytes 24580
  167.9 6.1 %copy-start.9 = (f32[1,12,64]{2,0,1:T(1,128)S(1)}, f32[1,12,64]{2,0,1:T(1,128)}, u32[]{:S(2)}) copy-start(f32[1,12,64]{2,0,1:T(1,128)} %get-tuple-element.39) | copy-start | bytes 9220
  169.0 5.6 %copy-start.11 = (f32[128]{0:T(128)S(1)}, f32[128]{0:T(128)}, u32[]{:S(2)}) copy-start(f32[128]{0:T(128)} %get-tuple-element.46) | copy-start | bytes 1540
  174.7 28.8 %copy-start.8 = (f32[12,128]{1,0:T(8,128)S(1)}, f32[12,128]{1,0:T(8,128)}, u32[]{:S(2)}) copy-start(f32[12,128]{1,0:T(8,128)} %copy-done.7) | copy-start | bytes 18436
  180.8 14.9 %all-to-all-start.5 = ((bf16[32,6,512]{2,1,0:T(8,128)(2,1)}), bf16[32,6,512]{2,1,0:T(8,128)(2,1)S(1)}, u32[]{:S(2)}, u32[]{:S(2)}) async-start(bf16[32,6,512]{2,1,0:T(8,128)(2,1)} %copy.151), calls=%async_computation.5 | async-start | bytes 524288 | tf_op jit(solution)/shard_map/local_sum/all_to_all | solution.py:26
  196.4 29.7 %all-to-all-start.6 = ((bf16[8,3,512]{2,1,0:T(4,128)(2,1)}), bf16[8,3,512]{2,1,0:T(4,128)(2,1)S(1)}, u32[]{:S(2)}, u32[]{:S(2)}) async-start(bf16[8,3,512]{2,1,0:T(4,128)(2,1)} %slice_reduce_fusion), calls=%async_computation.6 | async-start | bytes 65536 | tf_op jit(solution)/shard_map/far_scatter/all_to_all | solution.py:26

commit v3 on v2

v3 whole, which is shorter than its diff:
```python
import jax
import jax.numpy as jnp
from jax import lax
from jax.sharding import Mesh, PartitionSpec as P


D = 4096
HEAD_KEY = 64
VALUE_CHANNELS = 128
NEAR = 4
CORES = 2


epsilon = 1e-06
softness_factor = 16.0

TP = ("far", "near")
DP = ("x", "core")


def size_of(axes):
    return lax.psum(1, axes)


def exchange(blocks, axes):
    return lax.all_to_all(blocks, axes, split_axis=0, concat_axis=0, tiled=True)


def copies(value, axes):
    return exchange(jnp.broadcast_to(value[None], (size_of(axes), *value.shape)), axes)


def summed(blocks):
    return blocks.astype(jnp.float32).sum(axis=0)


def dot(left, right):
    return jnp.dot(left, right, preferred_element_type=jnp.float32)


def from_ring(value, held_for):
    n = size_of("x")
    onward = [(i, (i + 1) % n) for i in range(n)]
    back = [(i, (i - 1) % n) for i in range(n)]
    half = value.shape[0] // 2
    found = {0: value}
    ahead = behind = value
    for step in range(1, n // 2):
        found[step] = ahead = lax.ppermute(ahead, "x", onward)
        found[n - step] = behind = lax.ppermute(behind, "x", back)
    if held_for is not None:
        (ahead, behind), held_for = lax.optimization_barrier(((ahead, behind), held_for))
    found[n // 2] = jnp.concatenate(
        [lax.ppermute(ahead[:half], "x", onward), lax.ppermute(behind[half:], "x", back)],
        axis=0,
    )
    return jnp.stack([found[i] for i in range(n)]), held_for


def from_all(value, held_for=None):
    ours, held_for = from_ring(value, held_for)
    theirs = lax.ppermute(ours, "core", [(0, 1), (1, 0)])
    return (ours, theirs), held_for


def own_core_first(blocks, axis):
    return jnp.where(lax.axis_index("core") == 0, blocks, jnp.flip(blocks, axis))


def three_terms(value):
    terms = []
    for _ in range(3):
        term = lax.reduce_precision(value, 8, 7)
        terms.append(term.astype(jnp.bfloat16))
        value = value - term
    return terms


def mixed_over_time(projected, squares, decay_offset, state, out_gain):
    seq_rows, local_heads = state.shape[:2]
    key_cols = local_heads * HEAD_KEY
    value_cols = local_heads * VALUE_CHANNELS
    projected = projected * lax.rsqrt(squares / D + epsilon)[:, None]
    value_rows = projected[:, :value_cols].reshape(seq_rows, local_heads, VALUE_CHANNELS)
    gate_rows = projected[:, value_cols : 2 * value_cols].reshape(
        seq_rows, local_heads, VALUE_CHANNELS
    )
    rest = projected[:, 2 * value_cols :]
    query_rows = rest[:, :key_cols].reshape(seq_rows, local_heads, HEAD_KEY)
    key_rows = rest[:, key_cols : 2 * key_cols].reshape(
        seq_rows, local_heads, HEAD_KEY
    ) * HEAD_KEY ** (-0.5)
    decay_logits = rest[:, 2 * key_cols : 3 * key_cols]
    decay_logarithm = jax.nn.log_sigmoid(decay_logits) / softness_factor + decay_offset
    decay_rate = jnp.exp(decay_logarithm).reshape(seq_rows, local_heads, HEAD_KEY)
    fresh = (
        decay_rate[:, :, :, None] * state + key_rows[:, :, :, None] * value_rows[:, :, None, :]
    )
    readout = jnp.sum(query_rows[:, :, :, None] * fresh, axis=2)
    normed = readout * lax.rsqrt(jnp.mean(readout * readout, axis=2, keepdims=True) + epsilon)
    normed = normed * out_gain.reshape(local_heads, VALUE_CHANNELS)[None]
    gated_out = (normed * jax.nn.silu(gate_rows)).reshape(seq_rows, value_cols)
    return gated_out.astype(jnp.bfloat16), fresh


def per_device(
    hidden_in,
    input_norm_gain,
    w_query,
    w_key,
    w_decay,
    w_value,
    w_gate,
    out_gain,
    w_out,
    decay_offset,
    state,
):
    seq_rows = state.shape[1]
    value_cols = w_out.shape[1]
    own_rows, features = hidden_in.shape
    n_dp = size_of(DP)
    matrices = (w_value, w_gate, w_query, w_key, w_decay)

    hidden = copies(hidden_in, TP).reshape(-1, features)
    out_first, _ = from_all(w_out[0])
    rows = jnp.concatenate(
        [
            *(matrix[1].T for matrix in matrices),
            jnp.stack(three_terms(input_norm_gain[1])),
            jnp.zeros((13, features), jnp.bfloat16),
        ],
        axis=0,
    )

    widened = hidden.astype(jnp.float32)
    scaled = (widened * input_norm_gain[0][None, :]).astype(jnp.bfloat16)
    partial_value = [dot(scaled, matrix[0]).astype(jnp.bfloat16) for matrix in matrices]
    used = sum(part.shape[1] for part in partial_value)
    sent = jnp.concatenate([hidden, *partial_value], axis=1)
    arrived = exchange(sent.reshape(n_dp, seq_rows, -1), DP)
    fetched, arrived = from_all(rows, arrived)
    before = arrived[:, :, :features]
    own = before.astype(jnp.float32)
    gated_out, fresh_first = mixed_over_time(
        summed(arrived[:, :, features:]),
        jnp.sum(own * own, axis=(0, 2)),
        decay_offset[0],
        state[0],
        out_gain[0],
    )

    n_x = size_of("x")
    place, near = lax.axis_index("x"), lax.axis_index("near")
    head_terms = jnp.stack(
        [jnp.stack([dot(gated_out, part[i]) for part in out_first]) for i in range(n_x)]
    ).astype(jnp.bfloat16)
    near_sum = summed(exchange(head_terms, "near"))
    far_sum = summed(copies(near_sum.astype(jnp.bfloat16), "far"))
    before = lax.dynamic_index_in_dim(
        before.reshape(n_x, -1, seq_rows, features),
        lax.rem(place - near + n_x, n_x),
        0,
        keepdims=False,
    )
    after = own_core_first(before, 0).astype(jnp.float32) + far_sum
    hidden = copies(after.astype(jnp.bfloat16), "near")

    widened = hidden.astype(jnp.float32)
    projected = 0.0
    for i, part in enumerate(fetched):
        gain = summed(jnp.moveaxis(part[:, used : used + 3], 1, 0))
        scaled = (widened[:, i] * gain[:, None, :]).astype(jnp.bfloat16)
        projected = projected + lax.dot_general(
            scaled,
            part[:, :used],
            (((0, 2), (0, 2)), ((), ())),
            preferred_element_type=jnp.float32,
        )
    gated_out, fresh_second = mixed_over_time(
        projected,
        jnp.sum(widened * widened, axis=(0, 1, 3)),
        decay_offset[1],
        state[1],
        out_gain[1],
    )
    kept = lax.dynamic_slice_in_dim(hidden, near * own_rows, own_rows, 2)
    kept = own_core_first(kept, 1)
    kept = jnp.concatenate(
        [
            lax.dynamic_index_in_dim(kept, lax.rem(place - i + n_x, n_x), 0, keepdims=False)
            for i in range(n_x)
        ]
    ).reshape(n_dp, -1, value_cols)
    sent = jnp.concatenate(
        [jnp.broadcast_to(gated_out[None], (n_dp, *gated_out.shape)), kept], axis=1
    )
    arrived = exchange(sent, DP)
    head_terms = dot(arrived[:, :seq_rows].reshape(-1, value_cols), w_out[1])
    mixed = summed(exchange(head_terms.astype(jnp.bfloat16).reshape(-1, own_rows, features), TP))
    before = lax.dynamic_index_in_dim(
        arrived[:, seq_rows:], lax.axis_index("far"), 0, keepdims=False
    ).reshape(own_rows, features)
    hidden_out = (before.astype(jnp.float32) + mixed).astype(jnp.bfloat16)
    return (hidden_out, jnp.stack([fresh_first, fresh_second]))


def solution(mesh):
    sizes = mesh.shape
    fine = Mesh(
        mesh.devices.reshape(sizes["grp"], sizes["tp"] // NEAR, NEAR, sizes["dp"] // CORES, CORES),
        ("grp", *TP, *DP),
    )

    return jax.shard_map(
        per_device,
        mesh=fine,
        in_specs=(
            P(("grp", *TP), DP),
            P(None, DP),
            P(None, DP, TP),
            P(None, DP, TP),
            P(None, DP, TP),
            P(None, DP, TP),
            P(None, DP, TP),
            P(None, TP),
            P(None, TP, DP),
            P(None, ("grp", *DP), TP),
            P(None, ("grp", *DP), TP, None, None),
        ),
        out_specs=(P(("grp", *TP), DP), P(None, ("grp", *DP), TP, None, None)),
        check_vma=False,
    )
```

time: 228 us -> 229 us (level)
  blocking collectives: 0 us -> 7.97 us
    all_to_all x7 -> x6, waiting for transfers between devices: 67.8 us -> 77.7 us  [exchange(): return lax.all_to_all(blocks, axes, split_axis=0, concat_axis=0, tiled=True)]
    all_to_all x0 -> x1, blocking collectives: none -> 7.97 us  [exchange(): return lax.all_to_all(blocks, axes, split_axis=0, concat_axis=0, tiled=True)]
    ppermute x2, waiting for transfers between devices: 5.95 us -> 0.35 us  [from_ring(): found[step] = ahead = lax.ppermute(ahead, 'x', onward)]
    ppermute x6, waiting for transfers between devices: 4.93 us -> 0.02 us  [the longest x2 0.01 us: from_ring(): lax.ppermute(behind[half:], 'x', back)]
    squeeze x3 -> x0, local copies, waits for them, and re-layouts: 2.57 us -> none  [the longest x2 1.51 us: per_device(): matrix[1]]
    all_to_all x7 -> x6, starting transfers between devices: 75.5 us -> 73.3 us  [exchange(): return lax.all_to_all(blocks, axes, split_axis=0, concat_axis=0, tiled=True)]
    dot_general x21 -> x14, matrix products: 7.45 us -> 6.83 us  [dot(): return jnp.dot(left, right, preferred_element_type=jnp.float32)]
  transfers between devices with their start and end apart: 17 -> 16, of which waited for: 9 -> 6; matrix products, arithmetic and copies ran while one was open for 10% -> 8% of each run, Pallas kernels for 0% -> 0%
where the time goes in v3:
time: 229 us; the launch traced here: 228 us
  starting transfers between devices  106 us (46%)
  waiting for transfers between devices  78 us (34%)
  local copies, waits for them, and re-layouts  14.2 us (6%)
  other arithmetic  10.9 us (5%)
  matrix products  9.5 us (4%)
  blocking collectives  7.97 us (3%)
    all_to_all x6, waiting for transfers between devices, exchange(): return lax.all_to_all(blocks, axes, split_axis=0, concat_axis=0, tiled=True)  77.7 us
    all_to_all x6, starting transfers between devices, exchange(): return lax.all_to_all(blocks, axes, split_axis=0, concat_axis=0, tiled=True)  73.3 us
    ppermute x2, starting transfers between devices, from_ring(): lax.ppermute(behind[half:], 'x', back)  9.73 us
    ppermute x2, starting transfers between devices, from_ring(): found[n - step] = behind = lax.ppermute(behind, 'x', back)  8.31 us
    all_to_all x1, blocking collectives, exchange(): return lax.all_to_all(blocks, axes, split_axis=0, concat_axis=0, tiled=True)  7.97 us
    dot_general x14, matrix products, dot(): return jnp.dot(left, right, preferred_element_type=jnp.float32)  6.83 us
    ppermute x2, starting transfers between devices, from_ring(): found[step] = ahead = lax.ppermute(ahead, 'x', onward)  5.92 us
  transfers between devices with their start and end apart: 16, of which 6 were waited for; matrix products, arithmetic and copies ran while one was open for 8% of the time, Pallas kernels for 0%

profile of v3, /device:TPU:40, one launch (start us, length us, event | category | flops | bytes accessed | tf_op | source)
XLA Modules:
  0.0 227.9 jit_solution(15039973152569959773)
XLA Ops:
  2.5 1.0 slice.153
  5.6 3.6 %collective-permute-start = (bf16[464,512]{1,0:T(8,128)(2,1)S(1)}, bf16[464,512]{1,0:T(8,128)(2,1)S(1)}, u32[]{:S(2)}, u32[]{:S(2)}) collective-permute-start(bf16[464,512]{1,0:T(8,128)(2,1)S(1)} %concatenate.40), channel_id=1, source_target_pairs={{0,2},{2,4},{4,6},{6,0},{1,3},{3,5},{5,7},{7,1},{8,10},{10,12},{12... | collective-permute-start | bytes 1425416 | tf_op jit(solution)/shard_map/ppermute | solution.py:49
  9.2 3.5 %collective-permute-start.1 = (bf16[464,512]{1,0:T(8,128)(2,1)S(1)}, bf16[464,512]{1,0:T(8,128)(2,1)S(1)}, u32[]{:S(2)}, u32[]{:S(2)}) collective-permute-start(bf16[464,512]{1,0:T(8,128)(2,1)S(1)} %concatenate.40), channel_id=1, source_target_pairs={{0,6},{2,0},{4,2},{6,4},{1,7},{3,1},{5,3},{7,5},{8,14},{10,8},{12,... | collective-permute-start | bytes 1425416 | tf_op jit(solution)/shard_map/ppermute | solution.py:50
  13.5 45.8 %all-to-all-start = ((bf16[32,3,512]{2,1,0:T(4,128)(2,1)}), bf16[32,3,512]{2,1,0:T(4,128)(2,1)S(1)}, u32[]{:S(2)}, u32[]{:S(2)}) async-start(bf16[32,3,512]{2,1,0:T(4,128)(2,1)} %broadcast_in_dim.11), calls=%async_computation | async-start | bytes 262144 | tf_op jit(solution)/shard_map/all_to_all | solution.py:26
  59.3 2.4 %collective-permute-start.2 = (bf16[128,512]{1,0:T(8,128)(2,1)S(1)}, bf16[128,512]{1,0:T(8,128)(2,1)S(1)}, u32[]{:S(2)}, u32[]{:S(2)}) collective-permute-start(bf16[128,512]{1,0:T(8,128)(2,1)S(1)} %get-tuple-element.11), channel_id=1, source_target_pairs={{0,2},{2,4},{4,6},{6,0},{1,3},{3,5},{5,7},{7,1},{8,10},{10,12},{12... | collective-permute-start | bytes 393224 | tf_op jit(solution)/shard_map/ppermute | solution.py:49
  61.6 4.8 %collective-permute-start.4 = (bf16[128,512]{1,0:T(8,128)(2,1)S(1)}, bf16[128,512]{1,0:T(8,128)(2,1)S(1)}, u32[]{:S(2)}, u32[]{:S(2)}) collective-permute-start(bf16[128,512]{1,0:T(8,128)(2,1)S(1)} %get-tuple-element.11), channel_id=1, source_target_pairs={{0,6},{2,0},{4,2},{6,4},{1,7},{3,1},{5,3},{7,5},{8,14},{10,8},{12,... | collective-permute-start | bytes 393224 | tf_op jit(solution)/shard_map/ppermute | solution.py:50
  67.4 1.9 collective-permute-start.3
  70.6 5.2 %collective-permute-start.5 = (bf16[64,512]{1,0:T(8,128)(2,1)}, bf16[64,512]{1,0:T(8,128)(2,1)}, u32[]{:S(2)}, u32[]{:S(2)}) collective-permute-start(bf16[64,512]{1,0:T(8,128)(2,1)} %slice.206), channel_id=1, source_target_pairs={{0,6},{2,0},{4,2},{6,4},{1,7},{3,1},{5,3},{7,5},{8,14},{10,8},{12,... | collective-permute-start | bytes 196616 | tf_op jit(solution)/shard_map/ppermute | solution.py:54
  75.7 13.9 %all-to-all-done = bf16[32,3,512]{2,1,0:T(4,128)(2,1)S(1)} async-done(((bf16[32,3,512]{2,1,0:T(4,128)(2,1)}), bf16[32,3,512]{2,1,0:T(4,128)(2,1)S(1)}, u32[]{:S(2)}, u32[]{:S(2)}) %all-to-all-start) | async-done | bytes 98336 | tf_op jit(solution)/shard_map/all_to_all | solution.py:26
  94.7 3.6 %all-to-all-start.1 = ((bf16[8,12,960]{2,1,0:T(8,128)(2,1)}), bf16[8,12,960]{2,1,0:T(8,128)(2,1)S(1)}, u32[]{:S(2)}, u32[]{:S(2)}) async-start(bf16[8,12,960]{2,1,0:T(8,128)(2,1)} %concatenate.47), calls=%async_computation.1 | async-start | bytes 524288 | tf_op jit(solution)/shard_map/all_to_all | solution.py:26
  100.0 2.1 collective-permute-start.6
  102.2 3.4 %all-to-all-done.1 = bf16[8,12,960]{2,1,0:T(8,128)(2,1)S(1)} async-done(((bf16[8,12,960]{2,1,0:T(8,128)(2,1)}), bf16[8,12,960]{2,1,0:T(8,128)(2,1)S(1)}, u32[]{:S(2)}, u32[]{:S(2)}) %all-to-all-start.1) | async-done | bytes 184352 | tf_op jit(solution)/shard_map/all_to_all | solution.py:26
  107.5 1.0 fusion.17
  108.5 1.0 fusion.19
  109.7 1.0 fusion.21
  110.8 1.0 fusion.23
  112.8 3.4 %all-to-all-start.2 = ((bf16[4,2,12,512]{3,1,2,0:T(2,128)(2,1)}), bf16[4,2,12,512]{3,1,2,0:T(2,128)(2,1)S(1)}, u32[]{:S(2)}, u32[]{:S(2)}) async-start(bf16[4,2,12,512]{3,1,2,0:T(2,128)(2,1)} %copy.46), calls=%async_computation.2 | async-start | bytes 196608 | tf_op jit(solution)/shard_map/all_to_all | solution.py:26
  116.2 2.5 %collective-permute-start.7 = (bf16[232,512]{1,0:T(8,128)(2,1)S(1)}, bf16[232,512]{1,0:T(8,128)(2,1)S(1)}, u32[]{:S(2)}, u32[]{:S(2)}) collective-permute-start(bf16[232,512]{1,0:T(8,128)(2,1)S(1)} %slice.182), channel_id=1, source_target_pairs={{0,2},{2,4},{4,6},{6,0},{1,3},{3,5},{5,7},{7,1},{8,10},{10,12},{12... | collective-permute-start | bytes 712712 | tf_op jit(solution)/shard_map/ppermute | solution.py:54
  118.8 4.6 %collective-permute-start.8 = (bf16[232,512]{1,0:T(8,128)(2,1)S(1)}, bf16[232,512]{1,0:T(8,128)(2,1)}, u32[]{:S(2)}, u32[]{:S(2)}) collective-permute-start(bf16[232,512]{1,0:T(8,128)(2,1)S(1)} %slice.183), channel_id=1, source_target_pairs={{0,6},{2,0},{4,2},{6,4},{1,7},{3,1},{5,3},{7,5},{8,14},{10,8},{12,... | collective-permute-start | bytes 712712 | tf_op jit(solution)/shard_map/ppermute | solution.py:54
  124.3 7.0 %all-to-all-start.3 = ((bf16[8,2,12,512]{3,1,2,0:T(2,128)(2,1)}), bf16[8,2,12,512]{3,1,2,0:T(2,128)(2,1)}, u32[]{:S(2)}, u32[]{:S(2)}) async-start(bf16[8,2,12,512]{3,1,2,0:T(2,128)(2,1)} %broadcast_in_dim.12), calls=%async_computation.3 | async-start | bytes 393216 | tf_op jit(solution)/shard_map/all_to_all | solution.py:26
  131.3 1.0 maximum_bitcast_fusion
  132.3 1.4 pad_maximum_fusion
  133.7 2.0 collective-permute-start.9
  136.0 26.0 %all-to-all-done.3 = bf16[8,2,12,512]{3,1,2,0:T(2,128)(2,1)} async-done(((bf16[8,2,12,512]{3,1,2,0:T(2,128)(2,1)}), bf16[8,2,12,512]{3,1,2,0:T(2,128)(2,1)}, u32[]{:S(2)}, u32[]{:S(2)}) %all-to-all-start.3) | async-done | bytes 196640 | tf_op jit(solution)/shard_map/all_to_all | solution.py:26
  162.0 1.1 convert_reduce_fusion
  163.8 6.5 %all-to-all-start.4 = ((bf16[4,2,12,512]{3,1,2,0:T(2,128)(2,1)}), bf16[4,2,12,512]{3,1,2,0:T(2,128)(2,1)S(1)}, u32[]{:S(2)}, u32[]{:S(2)}) async-start(bf16[4,2,12,512]{3,1,2,0:T(2,128)(2,1)} %broadcast_in_dim.13), calls=%async_computation.4 | async-start | bytes 196608 | tf_op jit(solution)/shard_map/all_to_all | solution.py:26
  171.2 5.0 %all-to-all-done.4 = bf16[4,2,12,512]{3,1,2,0:T(2,128)(2,1)S(1)} async-done(((bf16[4,2,12,512]{3,1,2,0:T(2,128)(2,1)}), bf16[4,2,12,512]{3,1,2,0:T(2,128)(2,1)S(1)}, u32[]{:S(2)}, u32[]{:S(2)}) %all-to-all-start.4) | async-done | bytes 98336 | tf_op jit(solution)/shard_map/all_to_all | solution.py:26
  176.7 2.1 fusion.7
  180.6 8.0 %all_to_all.35 = bf16[8,24,128]{2,1,0:T(8,128)(2,1)S(1)} all-to-all(bf16[8,24,128]{2,1,0:T(8,128)(2,1)S(1)} %maximum_maximum_fusion), channel_id=1, replica_groups=mesh['grp'=2,'far'=8,'near'=4,'x'=4,'core'=2] {'x','core'}, dimensions={0} | all-to-all | bytes 98304 | tf_op jit(solution)/shard_map/all_to_all | solution.py:26
  189.5 7.0 %all-to-all-start.6 = ((bf16[32,3,512]{2,1,0:T(4,128)(2,1)}), bf16[32,3,512]{2,1,0:T(4,128)(2,1)S(1)}, u32[]{:S(2)}, u32[]{:S(2)}) async-start(bf16[32,3,512]{2,1,0:T(4,128)(2,1)} %reshape.246), calls=%async_computation.6 | async-start | bytes 262144 | tf_op jit(solution)/shard_map/all_to_all | solution.py:26
  196.9 0.9 pad_maximum_fusion.1
  197.9 29.3 %all-to-all-done.6 = bf16[32,3,512]{2,1,0:T(4,128)(2,1)S(1)} async-done(((bf16[32,3,512]{2,1,0:T(4,128)(2,1)}), bf16[32,3,512]{2,1,0:T(4,128)(2,1)S(1)}, u32[]{:S(2)}, u32[]{:S(2)}) %all-to-all-start.6) | async-done | bytes 98336 | tf_op jit(solution)/shard_map/all_to_all | solution.py:26
  (144 shorter events, 23.4 us)
Async XLA Ops:
  0.6 12.1 %copy-start.12 = (bf16[3,512]{1,0:T(4,128)(2,1)S(1)}, bf16[3,512]{1,0:T(4,128)(2,1)}, u32[]{:S(2)}) copy-start(bf16[3,512]{1,0:T(4,128)(2,1)} %param.11) | copy-start | bytes 9220
  0.6 58.6 %copy-start.3 = (bf16[2,128,512]{2,1,0:T(8,128)(2,1)S(1)}, bf16[2,128,512]{2,1,0:T(8,128)(2,1)}, u32[]{:S(2)}) copy-start(bf16[2,128,512]{2,1,0:T(8,128)(2,1)} %param.19) | copy-start | bytes 786436
  0.7 65.8 %copy-start.11 = (f32[2,12,64]{2,0,1:T(2,128)S(1)}, f32[2,12,64]{2,0,1:T(2,128)}, u32[]{:S(2)}) copy-start(f32[2,12,64]{2,0,1:T(2,128)} %param.20) | copy-start | bytes 18436
  0.7 68.7 %copy-start.15 = (f32[2,128]{1,0:T(2,128)S(1)}, f32[2,128]{1,0:T(2,128)}, u32[]{:S(2)}) copy-start(f32[2,128]{1,0:T(2,128)} %param.18) | copy-start | bytes 3076
  2.4 87.5 %copy-start.7 = (bf16[2,512,64]{1,2,0:T(8,128)(2,1)S(1)}, bf16[2,512,64]{1,2,0:T(8,128)(2,1)}, u32[]{:S(2)}) copy-start(bf16[2,512,64]{1,2,0:T(8,128)(2,1)} %param.13) | copy-start | bytes 393220
  2.5 88.1 %copy-start.5 = (bf16[2,512,128]{2,1,0:T(8,128)(2,1)S(1)}, bf16[2,512,128]{2,1,0:T(8,128)(2,1)}, u32[]{:S(2)}) copy-start(bf16[2,512,128]{2,1,0:T(8,128)(2,1)} %param.16) | copy-start | bytes 786436
  3.5 87.3 %copy-start.6 = (bf16[2,512,128]{2,1,0:T(8,128)(2,1)S(1)}, bf16[2,512,128]{2,1,0:T(8,128)(2,1)}, u32[]{:S(2)}) copy-start(bf16[2,512,128]{2,1,0:T(8,128)(2,1)} %param.17) | copy-start | bytes 786436
  3.6 87.4 %copy-start.8 = (bf16[2,512,64]{1,2,0:T(8,128)(2,1)S(1)}, bf16[2,512,64]{1,2,0:T(8,128)(2,1)}, u32[]{:S(2)}) copy-start(bf16[2,512,64]{1,2,0:T(8,128)(2,1)} %param.14) | copy-start | bytes 393220
  4.5 87.3 %copy-start.9 = (bf16[2,512,64]{1,2,0:T(8,128)(2,1)S(1)}, bf16[2,512,64]{1,2,0:T(8,128)(2,1)}, u32[]{:S(2)}) copy-start(bf16[2,512,64]{1,2,0:T(8,128)(2,1)} %param.15) | copy-start | bytes 393220
  5.6 96.5 %collective-permute-start = (bf16[464,512]{1,0:T(8,128)(2,1)S(1)}, bf16[464,512]{1,0:T(8,128)(2,1)S(1)}, u32[]{:S(2)}, u32[]{:S(2)}) collective-permute-start(bf16[464,512]{1,0:T(8,128)(2,1)S(1)} %concatenate.40), channel_id=1, source_target_pairs={{0,2},{2,4},{4,6},{6,0},{1,3},{3,5},{5,7},{7,1},{8,10},{10,12},{12... | collective-permute-start | bytes 1425416 | tf_op jit(solution)/shard_map/ppermute | solution.py:49
  9.2 92.9 %collective-permute-start.1 = (bf16[464,512]{1,0:T(8,128)(2,1)S(1)}, bf16[464,512]{1,0:T(8,128)(2,1)S(1)}, u32[]{:S(2)}, u32[]{:S(2)}) collective-permute-start(bf16[464,512]{1,0:T(8,128)(2,1)S(1)} %concatenate.40), channel_id=1, source_target_pairs={{0,6},{2,0},{4,2},{6,4},{1,7},{3,1},{5,3},{7,5},{8,14},{10,8},{12,... | collective-permute-start | bytes 1425416 | tf_op jit(solution)/shard_map/ppermute | solution.py:50
  13.5 76.2 %all-to-all-start = ((bf16[32,3,512]{2,1,0:T(4,128)(2,1)}), bf16[32,3,512]{2,1,0:T(4,128)(2,1)S(1)}, u32[]{:S(2)}, u32[]{:S(2)}) async-start(bf16[32,3,512]{2,1,0:T(4,128)(2,1)} %broadcast_in_dim.11), calls=%async_computation | async-start | bytes 262144 | tf_op jit(solution)/shard_map/all_to_all | solution.py:26
  59.3 8.1 %collective-permute-start.2 = (bf16[128,512]{1,0:T(8,128)(2,1)S(1)}, bf16[128,512]{1,0:T(8,128)(2,1)S(1)}, u32[]{:S(2)}, u32[]{:S(2)}) collective-permute-start(bf16[128,512]{1,0:T(8,128)(2,1)S(1)} %get-tuple-element.11), channel_id=1, source_target_pairs={{0,2},{2,4},{4,6},{6,0},{1,3},{3,5},{5,7},{7,1},{8,10},{10,12},{12... | collective-permute-start | bytes 393224 | tf_op jit(solution)/shard_map/ppermute | solution.py:49
  61.6 8.3 %collective-permute-start.4 = (bf16[128,512]{1,0:T(8,128)(2,1)S(1)}, bf16[128,512]{1,0:T(8,128)(2,1)S(1)}, u32[]{:S(2)}, u32[]{:S(2)}) collective-permute-start(bf16[128,512]{1,0:T(8,128)(2,1)S(1)} %get-tuple-element.11), channel_id=1, source_target_pairs={{0,6},{2,0},{4,2},{6,4},{1,7},{3,1},{5,3},{7,5},{8,14},{10,8},{12,... | collective-permute-start | bytes 393224 | tf_op jit(solution)/shard_map/ppermute | solution.py:50
  67.4 8.3 %collective-permute-start.3 = (bf16[64,512]{1,0:T(8,128)(2,1)S(1)}, bf16[64,512]{1,0:T(8,128)(2,1)S(1)}, u32[]{:S(2)}, u32[]{:S(2)}) collective-permute-start(bf16[64,512]{1,0:T(8,128)(2,1)S(1)} %slice.205), channel_id=1, source_target_pairs={{0,2},{2,4},{4,6},{6,0},{1,3},{3,5},{5,7},{7,1},{8,10},{10,12},{12... | collective-permute-start | bytes 196616 | tf_op jit(solution)/shard_map/ppermute | solution.py:54
  70.6 27.7 %collective-permute-start.5 = (bf16[64,512]{1,0:T(8,128)(2,1)}, bf16[64,512]{1,0:T(8,128)(2,1)}, u32[]{:S(2)}, u32[]{:S(2)}) collective-permute-start(bf16[64,512]{1,0:T(8,128)(2,1)} %slice.206), channel_id=1, source_target_pairs={{0,6},{2,0},{4,2},{6,4},{1,7},{3,1},{5,3},{7,5},{8,14},{10,8},{12,... | collective-permute-start | bytes 196616 | tf_op jit(solution)/shard_map/ppermute | solution.py:54
  91.0 15.6 %copy-start = (f32[2,12,1,64,128]{4,3,2,1,0:T(8,128)S(1)}, f32[2,12,1,64,128]{4,3,2,1,0:T(8,128)}, u32[]{:S(2)}) copy-start(f32[2,12,1,64,128]{4,3,2,1,0:T(8,128)} %param.21) | copy-start | bytes 2359300
  92.7 14.4 %copy-start.14 = (f32[128]{0:T(128)S(1)}, f32[128]{0:T(128)}, u32[]{:S(2)}) copy-start(f32[128]{0:T(128)} %get-tuple-element.33) | copy-start | bytes 1540
  94.7 10.9 %all-to-all-start.1 = ((bf16[8,12,960]{2,1,0:T(8,128)(2,1)}), bf16[8,12,960]{2,1,0:T(8,128)(2,1)S(1)}, u32[]{:S(2)}, u32[]{:S(2)}) async-start(bf16[8,12,960]{2,1,0:T(8,128)(2,1)} %concatenate.47), calls=%async_computation.1 | async-start | bytes 524288 | tf_op jit(solution)/shard_map/all_to_all | solution.py:26
  100.0 7.5 %collective-permute-start.6 = (bf16[4,128,512]{2,1,0:T(8,128)(2,1)}, bf16[4,128,512]{2,1,0:T(8,128)(2,1)}, u32[]{:S(2)}, u32[]{:S(2)}) collective-permute-start(bf16[4,128,512]{2,1,0:T(8,128)(2,1)} %pad_maximum_fusion.2), channel_id=1, source_target_pairs={{0,1},{1,0},{2,3},{3,2},{4,5},{5,4},{6,7},{7,6},{8,9},{9,8},{10,11... | collective-permute-start | bytes 1572872 | tf_op jit(solution)/shard_map/ppermute | solution.py:62
  102.2 16.6 %copy-start.1 = (bf16[464,512]{1,0:T(8,128)(2,1)}, bf16[464,512]{1,0:T(8,128)(2,1)S(1)}, u32[]{:S(2)}) copy-start(bf16[464,512]{1,0:T(8,128)(2,1)S(1)} %collective-permute-done) | copy-start | bytes 1425412
  102.2 16.6 %copy-start.2 = (bf16[464,512]{1,0:T(8,128)(2,1)}, bf16[464,512]{1,0:T(8,128)(2,1)S(1)}, u32[]{:S(2)}) copy-start(bf16[464,512]{1,0:T(8,128)(2,1)S(1)} %collective-permute-done.1) | copy-start | bytes 1425412
  112.8 10.6 %all-to-all-start.2 = ((bf16[4,2,12,512]{3,1,2,0:T(2,128)(2,1)}), bf16[4,2,12,512]{3,1,2,0:T(2,128)(2,1)S(1)}, u32[]{:S(2)}, u32[]{:S(2)}) async-start(bf16[4,2,12,512]{3,1,2,0:T(2,128)(2,1)} %copy.46), calls=%async_computation.2 | async-start | bytes 196608 | tf_op jit(solution)/shard_map/all_to_all | solution.py:26
  116.2 15.1 %collective-permute-start.7 = (bf16[232,512]{1,0:T(8,128)(2,1)S(1)}, bf16[232,512]{1,0:T(8,128)(2,1)S(1)}, u32[]{:S(2)}, u32[]{:S(2)}) collective-permute-start(bf16[232,512]{1,0:T(8,128)(2,1)S(1)} %slice.182), channel_id=1, source_target_pairs={{0,2},{2,4},{4,6},{6,0},{1,3},{3,5},{5,7},{7,1},{8,10},{10,12},{12... | collective-permute-start | bytes 712712 | tf_op jit(solution)/shard_map/ppermute | solution.py:54
  118.8 12.5 %collective-permute-start.8 = (bf16[232,512]{1,0:T(8,128)(2,1)S(1)}, bf16[232,512]{1,0:T(8,128)(2,1)}, u32[]{:S(2)}, u32[]{:S(2)}) collective-permute-start(bf16[232,512]{1,0:T(8,128)(2,1)S(1)} %slice.183), channel_id=1, source_target_pairs={{0,6},{2,0},{4,2},{6,4},{1,7},{3,1},{5,3},{7,5},{8,14},{10,8},{12,... | collective-permute-start | bytes 712712 | tf_op jit(solution)/shard_map/ppermute | solution.py:54
  124.3 37.7 %all-to-all-start.3 = ((bf16[8,2,12,512]{3,1,2,0:T(2,128)(2,1)}), bf16[8,2,12,512]{3,1,2,0:T(2,128)(2,1)}, u32[]{:S(2)}, u32[]{:S(2)}) async-start(bf16[8,2,12,512]{3,1,2,0:T(2,128)(2,1)} %broadcast_in_dim.12), calls=%async_computation.3 | async-start | bytes 393216 | tf_op jit(solution)/shard_map/all_to_all | solution.py:26
  133.7 36.7 %collective-permute-start.9 = (bf16[4,464,512]{2,1,0:T(8,128)(2,1)S(1)}, bf16[4,464,512]{2,1,0:T(8,128)(2,1)}, u32[]{:S(2)}, u32[]{:S(2)}) collective-permute-start(bf16[4,464,512]{2,1,0:T(8,128)(2,1)S(1)} %pad_maximum_fusion), channel_id=1, source_target_pairs={{0,1},{1,0},{2,3},{3,2},{4,5},{5,4},{6,7},{7,6},{8,9},{9,8},{10,11... | collective-permute-start | bytes 5701640 | tf_op jit(solution)/shard_map/ppermute | solution.py:62
  163.8 12.4 %all-to-all-start.4 = ((bf16[4,2,12,512]{3,1,2,0:T(2,128)(2,1)}), bf16[4,2,12,512]{3,1,2,0:T(2,128)(2,1)S(1)}, u32[]{:S(2)}, u32[]{:S(2)}) async-start(bf16[4,2,12,512]{3,1,2,0:T(2,128)(2,1)} %broadcast_in_dim.13), calls=%async_computation.4 | async-start | bytes 196608 | tf_op jit(solution)/shard_map/all_to_all | solution.py:26
  176.7 2.7 %copy-start.10 = (f32[1,12,64]{2,0,1:T(1,128)S(1)}, f32[1,12,64]{2,0,1:T(1,128)}, u32[]{:S(2)}) copy-start(f32[1,12,64]{2,0,1:T(1,128)} %get-tuple-element.26) | copy-start | bytes 9220
  178.8 1.7 copy-start.13
  178.8 9.8 %copy-start.4 = (bf16[2,128,512]{2,1,0:T(8,128)(2,1)S(1)}, bf16[2,128,512]{2,1,0:T(8,128)(2,1)}, u32[]{:S(2)}) copy-start(bf16[2,128,512]{2,1,0:T(8,128)(2,1)} %param.19) | copy-start | bytes 786436
  189.5 37.7 %all-to-all-start.6 = ((bf16[32,3,512]{2,1,0:T(4,128)(2,1)}), bf16[32,3,512]{2,1,0:T(4,128)(2,1)S(1)}, u32[]{:S(2)}, u32[]{:S(2)}) async-start(bf16[32,3,512]{2,1,0:T(4,128)(2,1)} %reshape.246), calls=%async_computation.6 | async-start | bytes 262144 | tf_op jit(solution)/shard_map/all_to_all | solution.py:26

commit v4 on v3

--- a/solution.py
+++ b/solution.py
@@ -38,29 +38,29 @@
     return jnp.dot(left, right, preferred_element_type=jnp.float32)
 
 
-def from_ring(value, held_for):
+def from_ring(value):
     n = size_of("x")
-    onward = [(i, (i + 1) % n) for i in range(n)]
-    back = [(i, (i - 1) % n) for i in range(n)]
     half = value.shape[0] // 2
+
+    def onward(part):
+        return lax.ppermute(part, "x", [(i, (i + 1) % n) for i in range(n)])
+
+    def back(part):
+        return lax.ppermute(part, "x", [(i, (i - 1) % n) for i in range(n)])
+
     found = {0: value}
     ahead = behind = value
     for step in range(1, n // 2):
-        found[step] = ahead = lax.ppermute(ahead, "x", onward)
-        found[n - step] = behind = lax.ppermute(behind, "x", back)
-    if held_for is not None:
-        (ahead, behind), held_for = lax.optimization_barrier(((ahead, behind), held_for))
-    found[n // 2] = jnp.concatenate(
-        [lax.ppermute(ahead[:half], "x", onward), lax.ppermute(behind[half:], "x", back)],
-        axis=0,
-    )
-    return jnp.stack([found[i] for i in range(n)]), held_for
-
-
-def from_all(value, held_for=None):
-    ours, held_for = from_ring(value, held_for)
+        found[step] = ahead = onward(ahead)
+        found[n - step] = behind = back(behind)
+    found[n // 2] = jnp.concatenate([onward(ahead[:half]), back(behind[half:])], axis=0)
+    return jnp.stack([found[i] for i in range(n)])
+
+
+def from_all(value):
+    ours = from_ring(value)
     theirs = lax.ppermute(ours, "core", [(0, 1), (1, 0)])
-    return (ours, theirs), held_for
+    return ours, theirs
 
 
 def own_core_first(blocks, axis):
@@ -123,23 +123,25 @@
     matrices = (w_value, w_gate, w_query, w_key, w_decay)
 
     hidden = copies(hidden_in, TP).reshape(-1, features)
-    out_first, _ = from_all(w_out[0])
-    rows = jnp.concatenate(
-        [
-            *(matrix[1].T for matrix in matrices),
-            jnp.stack(three_terms(input_norm_gain[1])),
-            jnp.zeros((13, features), jnp.bfloat16),
-        ],
-        axis=0,
-    )
-
+    out_first = from_all(w_out[0])
     widened = hidden.astype(jnp.float32)
     scaled = (widened * input_norm_gain[0][None, :]).astype(jnp.bfloat16)
     partial_value = [dot(scaled, matrix[0]).astype(jnp.bfloat16) for matrix in matrices]
     used = sum(part.shape[1] for part in partial_value)
     sent = jnp.concatenate([hidden, *partial_value], axis=1)
     arrived = exchange(sent.reshape(n_dp, seq_rows, -1), DP)
-    fetched, arrived = from_all(rows, arrived)
+    weights, arrived = lax.optimization_barrier(
+        ([matrix[1] for matrix in matrices] + [input_norm_gain[1]], arrived)
+    )
+    rows = jnp.concatenate(
+        [
+            *(matrix.T for matrix in weights[:-1]),
+            jnp.stack(three_terms(weights[-1])),
+            jnp.zeros((13, features), jnp.bfloat16),
+        ],
+        axis=0,
+    )
+    fetched = from_all(rows)
     before = arrived[:, :, :features]
     own = before.astype(jnp.float32)
     gated_out, fresh_first = mixed_over_time(

time: 229 us -> 231 us (level)
  waiting for transfers between devices: 78 us -> 66.8 us
  blocking collectives: 7.97 us -> 17.9 us
  starting transfers between devices: 106 us -> 113 us
  matrix products: 9.5 us -> 4.64 us
  local copies, waits for them, and re-layouts: 14.2 us -> 17.5 us
  other arithmetic: 10.9 us -> 7.85 us
    all_to_all x6 -> x5, waiting for transfers between devices: 77.7 us -> 56.7 us  [exchange(): return lax.all_to_all(blocks, axes, split_axis=0, concat_axis=0, tiled=True)]
    all_to_all x1 -> x2, blocking collectives: 7.97 us -> 17.9 us  [exchange(): return lax.all_to_all(blocks, axes, split_axis=0, concat_axis=0, tiled=True)]
    ppermute x8, waiting for transfers between devices: 0.37 us -> 10.1 us  [the longest x4 8.66 us: onward(): return lax.ppermute(part, 'x', [(i, (i + 1) % n) for i in range(n)])]
    all_to_all x6 -> x5, starting transfers between devices: 73.3 us -> 80.5 us  [exchange(): return lax.all_to_all(blocks, axes, split_axis=0, concat_axis=0, tiled=True)]
    dot_general x14, matrix products: 6.83 us -> 1.99 us  [dot(): return jnp.dot(left, right, preferred_element_type=jnp.float32)]
    squeeze x0 -> x2, local copies, waits for them, and re-layouts: none -> 2.36 us  [per_device(): matrix[1]]
  transfers between devices with their start and end apart: 16 -> 15, of which waited for: 6 -> 8; matrix products, arithmetic and copies ran while one was open for 8% -> 9% of each run, Pallas kernels for 0% -> 0%
where the time goes in v4:
time: 231 us; the launch traced here: 229 us
  starting transfers between devices  113 us (49%)
  waiting for transfers between devices  66.8 us (29%)
  blocking collectives  17.9 us (8%)
  local copies, waits for them, and re-layouts  17.5 us (8%)
  other arithmetic  7.85 us (3%)
  matrix products  4.64 us (2%)
    all_to_all x5, starting transfers between devices, exchange(): return lax.all_to_all(blocks, axes, split_axis=0, concat_axis=0, tiled=True)  80.5 us
    all_to_all x5, waiting for transfers between devices, exchange(): return lax.all_to_all(blocks, axes, split_axis=0, concat_axis=0, tiled=True)  56.7 us
    ppermute x4, starting transfers between devices, back(): return lax.ppermute(part, 'x', [(i, (i - 1) % n) for i in range(n)])  18 us
    all_to_all x2, blocking collectives, exchange(): return lax.all_to_all(blocks, axes, split_axis=0, concat_axis=0, tiled=True)  17.9 us
    ppermute x4, starting transfers between devices, onward(): return lax.ppermute(part, 'x', [(i, (i + 1) % n) for i in range(n)])  10.5 us
    ppermute x4, waiting for transfers between devices, onward(): return lax.ppermute(part, 'x', [(i, (i + 1) % n) for i in range(n)])  8.66 us
  transfers between devices with their start and end apart: 15, of which 8 were waited for; matrix products, arithmetic and copies ran while one was open for 9% of the time, Pallas kernels for 0%

profile of v4, /device:TPU:40, one launch (start us, length us, event | category | flops | bytes accessed | tf_op | source)
XLA Modules:
  0.0 229.5 jit_solution(3608462018562381029)
XLA Ops:
  1.7 3.7 %collective-permute-start = (bf16[128,512]{1,0:T(8,128)(2,1)S(1)}, bf16[128,512]{1,0:T(8,128)(2,1)S(1)}, u32[]{:S(2)}, u32[]{:S(2)}) collective-permute-start(bf16[128,512]{1,0:T(8,128)(2,1)S(1)} %get-tuple-element.19), channel_id=1, source_target_pairs={{0,2},{2,4},{4,6},{6,0},{1,3},{3,5},{5,7},{7,1},{8,10},{10,12},{12... | collective-permute-start | bytes 393224 | tf_op jit(solution)/shard_map/ppermute | solution.py:46
  5.4 3.5 %collective-permute-start.2 = (bf16[128,512]{1,0:T(8,128)(2,1)S(1)}, bf16[128,512]{1,0:T(8,128)(2,1)S(1)}, u32[]{:S(2)}, u32[]{:S(2)}) collective-permute-start(bf16[128,512]{1,0:T(8,128)(2,1)S(1)} %get-tuple-element.19), channel_id=1, source_target_pairs={{0,6},{2,0},{4,2},{6,4},{1,7},{3,1},{5,3},{7,5},{8,14},{10,8},{12,... | collective-permute-start | bytes 393224 | tf_op jit(solution)/shard_map/ppermute | solution.py:49
  9.0 1.4 broadcast_in_dim.10
  10.3 45.8 %all-to-all-start = ((bf16[32,3,512]{2,1,0:T(4,128)(2,1)}), bf16[32,3,512]{2,1,0:T(4,128)(2,1)S(1)}, u32[]{:S(2)}, u32[]{:S(2)}) async-start(bf16[32,3,512]{2,1,0:T(4,128)(2,1)} %broadcast_in_dim.10), calls=%async_computation | async-start | bytes 262144 | tf_op jit(solution)/shard_map/all_to_all | solution.py:26
  57.0 1.5 slice_bitcast_fusion.8
  58.5 1.4 fusion.63
  60.6 2.4 %collective-permute-start.1 = (bf16[64,512]{1,0:T(8,128)(2,1)S(1)}, bf16[64,512]{1,0:T(8,128)(2,1)S(1)}, u32[]{:S(2)}, u32[]{:S(2)}) collective-permute-start(bf16[64,512]{1,0:T(8,128)(2,1)S(1)} %slice.205), channel_id=1, source_target_pairs={{0,2},{2,4},{4,6},{6,0},{1,3},{3,5},{5,7},{7,1},{8,10},{10,12},{12... | collective-permute-start | bytes 196616 | tf_op jit(solution)/shard_map/ppermute | solution.py:46
  63.0 1.3 slice_bitcast_fusion.11
  66.1 4.8 %collective-permute-start.3 = (bf16[64,512]{1,0:T(8,128)(2,1)S(1)}, bf16[64,512]{1,0:T(8,128)(2,1)S(1)}, u32[]{:S(2)}, u32[]{:S(2)}) collective-permute-start(bf16[64,512]{1,0:T(8,128)(2,1)S(1)} %slice.206), channel_id=1, source_target_pairs={{0,6},{2,0},{4,2},{6,4},{1,7},{3,1},{5,3},{7,5},{8,14},{10,8},{12,... | collective-permute-start | bytes 196616 | tf_op jit(solution)/shard_map/ppermute | solution.py:49
  70.9 15.7 %all-to-all-done = bf16[32,3,512]{2,1,0:T(4,128)(2,1)S(1)} async-done(((bf16[32,3,512]{2,1,0:T(4,128)(2,1)}), bf16[32,3,512]{2,1,0:T(4,128)(2,1)S(1)}, u32[]{:S(2)}, u32[]{:S(2)}) %all-to-all-start) | async-done | bytes 98336 | tf_op jit(solution)/shard_map/all_to_all | solution.py:26
  88.9 3.6 %all-to-all-start.1 = ((bf16[8,12,960]{2,1,0:T(8,128)(2,1)}), bf16[8,12,960]{2,1,0:T(8,128)(2,1)S(1)}, u32[]{:S(2)}, u32[]{:S(2)}) async-start(bf16[8,12,960]{2,1,0:T(8,128)(2,1)} %concatenate.46), calls=%async_computation.1 | async-start | bytes 524288 | tf_op jit(solution)/shard_map/all_to_all | solution.py:26
  92.7 2.1 collective-permute-start.4
  94.8 5.0 %all-to-all-done.1 = bf16[8,12,960]{2,1,0:T(8,128)(2,1)S(1)} async-done(((bf16[8,12,960]{2,1,0:T(8,128)(2,1)}), bf16[8,12,960]{2,1,0:T(8,128)(2,1)S(1)}, u32[]{:S(2)}, u32[]{:S(2)}) %all-to-all-start.1) | async-done | bytes 184352 | tf_op jit(solution)/shard_map/all_to_all | solution.py:26
  102.1 8.3 %all_to_all.35 = bf16[4,2,12,512]{3,1,2,0:T(2,128)(2,1)S(1)} all-to-all(bf16[4,2,12,512]{3,1,2,0:T(2,128)(2,1)S(1)} %copy.46), channel_id=1, replica_groups=mesh['grp'=2,'far'=8,'near'=4,'x'=4,'core'=2] {'near'}, dimensions={0} | all-to-all | bytes 196608 | tf_op jit(solution)/shard_map/all_to_all | solution.py:26
  111.2 5.3 %all-to-all-start.3 = ((bf16[8,2,12,512]{3,1,2,0:T(2,128)(2,1)}), bf16[8,2,12,512]{3,1,2,0:T(2,128)(2,1)S(1)}, u32[]{:S(2)}, u32[]{:S(2)}) async-start(bf16[8,2,12,512]{3,1,2,0:T(2,128)(2,1)} %broadcast_in_dim.11), calls=%async_computation.3 | async-start | bytes 393216 | tf_op jit(solution)/shard_map/all_to_all | solution.py:26
  116.6 2.8 %concatenate.48 = bf16[464,512]{1,0:T(8,128)(2,1)S(1)} concatenate(bf16[128,512]{1,0:T(8,128)(2,1)S(1)} %bitcast.154, bf16[128,512]{1,0:T(8,128)(2,1)} %bitcast.155, bf16[64,512]{1,0:T(8,128)(2,1)S(1)} %bitcast.156, bf16[64,512]{1,0:T(8,128)(2,1)} %bitcast.158, bf16[64,512]{1,0:T(8,128)(2,1)} %bitcast.157, bf16[1,512]{1,0:T(2,128)(2,1)S(1)} %stack.130, ...), dimensions={0} | concatenate | bytes 950272 | tf_op jit(solution)/shard_map/concatenate | solution.py:136
  119.4 2.5 %collective-permute-start.5 = (bf16[464,512]{1,0:T(8,128)(2,1)S(1)}, bf16[464,512]{1,0:T(8,128)(2,1)S(1)}, u32[]{:S(2)}, u32[]{:S(2)}) collective-permute-start(bf16[464,512]{1,0:T(8,128)(2,1)S(1)} %concatenate.48), channel_id=1, source_target_pairs={{0,2},{2,4},{4,6},{6,0},{1,3},{3,5},{5,7},{7,1},{8,10},{10,12},{12... | collective-permute-start | bytes 1425416 | tf_op jit(solution)/shard_map/ppermute | solution.py:46
  122.0 4.6 %collective-permute-start.7 = (bf16[464,512]{1,0:T(8,128)(2,1)S(1)}, bf16[464,512]{1,0:T(8,128)(2,1)S(1)}, u32[]{:S(2)}, u32[]{:S(2)}) collective-permute-start(bf16[464,512]{1,0:T(8,128)(2,1)S(1)} %concatenate.48), channel_id=1, source_target_pairs={{0,6},{2,0},{4,2},{6,4},{1,7},{3,1},{5,3},{7,5},{8,14},{10,8},{12,... | collective-permute-start | bytes 1425416 | tf_op jit(solution)/shard_map/ppermute | solution.py:49
  126.6 6.8 %collective-permute-done.5 = bf16[464,512]{1,0:T(8,128)(2,1)S(1)} collective-permute-done((bf16[464,512]{1,0:T(8,128)(2,1)S(1)}, bf16[464,512]{1,0:T(8,128)(2,1)S(1)}, u32[]{:S(2)}, u32[]{:S(2)}) %collective-permute-start.5) | collective-permute-done | bytes 475168 | tf_op jit(solution)/shard_map/ppermute | solution.py:46
  133.4 2.0 collective-permute-start.6
  135.4 5.2 %collective-permute-start.8 = (bf16[232,512]{1,0:T(8,128)(2,1)S(1)}, bf16[232,512]{1,0:T(8,128)(2,1)}, u32[]{:S(2)}, u32[]{:S(2)}) collective-permute-start(bf16[232,512]{1,0:T(8,128)(2,1)S(1)} %slice.213), channel_id=1, source_target_pairs={{0,6},{2,0},{4,2},{6,4},{1,7},{3,1},{5,3},{7,5},{8,14},{10,8},{12,... | collective-permute-start | bytes 712712 | tf_op jit(solution)/shard_map/ppermute | solution.py:49
  140.9 1.8 collective-permute-done.6
  142.8 1.4 collective-permute-done.8
  144.2 1.1 maximum_bitcast_fusion
  145.3 1.4 pad_maximum_fusion
  146.7 2.0 collective-permute-start.9
  150.6 3.4 %all-to-all-start.4 = ((bf16[4,2,12,512]{3,1,2,0:T(2,128)(2,1)}), bf16[4,2,12,512]{3,1,2,0:T(2,128)(2,1)S(1)}, u32[]{:S(2)}, u32[]{:S(2)}) async-start(bf16[4,2,12,512]{3,1,2,0:T(2,128)(2,1)} %broadcast_in_dim.12), calls=%async_computation.4 | async-start | bytes 196608 | tf_op jit(solution)/shard_map/all_to_all | solution.py:26
  154.1 5.7 %all-to-all-done.4 = bf16[4,2,12,512]{3,1,2,0:T(2,128)(2,1)S(1)} async-done(((bf16[4,2,12,512]{3,1,2,0:T(2,128)(2,1)}), bf16[4,2,12,512]{3,1,2,0:T(2,128)(2,1)S(1)}, u32[]{:S(2)}, u32[]{:S(2)}) %all-to-all-start.4) | async-done | bytes 98336 | tf_op jit(solution)/shard_map/all_to_all | solution.py:26
  161.5 2.1 fusion.7
  165.0 9.7 %all_to_all.36 = bf16[8,24,128]{2,1,0:T(8,128)(2,1)S(1)} all-to-all(bf16[8,24,128]{2,1,0:T(8,128)(2,1)S(1)} %maximum_maximum_fusion), channel_id=1, replica_groups=mesh['grp'=2,'far'=8,'near'=4,'x'=4,'core'=2] {'x','core'}, dimensions={0} | all-to-all | bytes 98304 | tf_op jit(solution)/shard_map/all_to_all | solution.py:26
  175.6 22.4 %all-to-all-start.6 = ((bf16[32,3,512]{2,1,0:T(4,128)(2,1)}), bf16[32,3,512]{2,1,0:T(4,128)(2,1)S(1)}, u32[]{:S(2)}, u32[]{:S(2)}) async-start(bf16[32,3,512]{2,1,0:T(4,128)(2,1)} %reshape.246), calls=%async_computation.6 | async-start | bytes 262144 | tf_op jit(solution)/shard_map/all_to_all | solution.py:26
  199.5 29.3 %all-to-all-done.6 = bf16[32,3,512]{2,1,0:T(4,128)(2,1)S(1)} async-done(((bf16[32,3,512]{2,1,0:T(4,128)(2,1)}), bf16[32,3,512]{2,1,0:T(4,128)(2,1)S(1)}, u32[]{:S(2)}, u32[]{:S(2)}) %all-to-all-start.6) | async-done | bytes 98336 | tf_op jit(solution)/shard_map/all_to_all | solution.py:26
  (152 shorter events, 18.2 us)
Async XLA Ops:
  0.6 86.1 %copy-start.7 = (bf16[2,512,64]{1,2,0:T(8,128)(2,1)S(1)}, bf16[2,512,64]{1,2,0:T(8,128)(2,1)}, u32[]{:S(2)}) copy-start(bf16[2,512,64]{1,2,0:T(8,128)(2,1)} %param.13) | copy-start | bytes 393220
  0.6 86.2 %copy-start.8 = (bf16[2,512,64]{1,2,0:T(8,128)(2,1)S(1)}, bf16[2,512,64]{1,2,0:T(8,128)(2,1)}, u32[]{:S(2)}) copy-start(bf16[2,512,64]{1,2,0:T(8,128)(2,1)} %param.14) | copy-start | bytes 393220
  0.7 86.4 %copy-start.6 = (bf16[2,512,128]{2,1,0:T(8,128)(2,1)S(1)}, bf16[2,512,128]{2,1,0:T(8,128)(2,1)}, u32[]{:S(2)}) copy-start(bf16[2,512,128]{2,1,0:T(8,128)(2,1)} %param.16) | copy-start | bytes 786436
  0.7 64.6 %slice-start = ((bf16[2,512,128]{2,1,0:T(8,128)(2,1)}), bf16[1,512,128]{2,1,0:T(8,128)(2,1)S(1)}, s32[]{:S(2)}) async-start(bf16[2,512,128]{2,1,0:T(8,128)(2,1)} %param.17), calls=%async_computation.7 | async-start | bytes 262144 | tf_op jit(solution)/shard_map/slice | solution.py:134
  0.7 86.5 %copy-start.5 = (bf16[2,512,128]{2,1,0:T(8,128)(2,1)S(1)}, bf16[2,512,128]{2,1,0:T(8,128)(2,1)}, u32[]{:S(2)}) copy-start(bf16[2,512,128]{2,1,0:T(8,128)(2,1)} %param.17) | copy-start | bytes 786436
  1.7 85.7 %copy-start.9 = (bf16[2,512,64]{1,2,0:T(8,128)(2,1)S(1)}, bf16[2,512,64]{1,2,0:T(8,128)(2,1)}, u32[]{:S(2)}) copy-start(bf16[2,512,64]{1,2,0:T(8,128)(2,1)} %param.15) | copy-start | bytes 393220
  1.7 58.9 %collective-permute-start = (bf16[128,512]{1,0:T(8,128)(2,1)S(1)}, bf16[128,512]{1,0:T(8,128)(2,1)S(1)}, u32[]{:S(2)}, u32[]{:S(2)}) collective-permute-start(bf16[128,512]{1,0:T(8,128)(2,1)S(1)} %get-tuple-element.19), channel_id=1, source_target_pairs={{0,2},{2,4},{4,6},{6,0},{1,3},{3,5},{5,7},{7,1},{8,10},{10,12},{12... | collective-permute-start | bytes 393224 | tf_op jit(solution)/shard_map/ppermute | solution.py:46
  5.4 60.7 %collective-permute-start.2 = (bf16[128,512]{1,0:T(8,128)(2,1)S(1)}, bf16[128,512]{1,0:T(8,128)(2,1)S(1)}, u32[]{:S(2)}, u32[]{:S(2)}) collective-permute-start(bf16[128,512]{1,0:T(8,128)(2,1)S(1)} %get-tuple-element.19), channel_id=1, source_target_pairs={{0,6},{2,0},{4,2},{6,4},{1,7},{3,1},{5,3},{7,5},{8,14},{10,8},{12,... | collective-permute-start | bytes 393224 | tf_op jit(solution)/shard_map/ppermute | solution.py:49
  10.3 76.2 %all-to-all-start = ((bf16[32,3,512]{2,1,0:T(4,128)(2,1)}), bf16[32,3,512]{2,1,0:T(4,128)(2,1)S(1)}, u32[]{:S(2)}, u32[]{:S(2)}) async-start(bf16[32,3,512]{2,1,0:T(4,128)(2,1)} %broadcast_in_dim.10), calls=%async_computation | async-start | bytes 262144 | tf_op jit(solution)/shard_map/all_to_all | solution.py:26
  60.6 10.2 %collective-permute-start.1 = (bf16[64,512]{1,0:T(8,128)(2,1)S(1)}, bf16[64,512]{1,0:T(8,128)(2,1)S(1)}, u32[]{:S(2)}, u32[]{:S(2)}) collective-permute-start(bf16[64,512]{1,0:T(8,128)(2,1)S(1)} %slice.205), channel_id=1, source_target_pairs={{0,2},{2,4},{4,6},{6,0},{1,3},{3,5},{5,7},{7,1},{8,10},{10,12},{12... | collective-permute-start | bytes 196616 | tf_op jit(solution)/shard_map/ppermute | solution.py:46
  66.1 26.4 %collective-permute-start.3 = (bf16[64,512]{1,0:T(8,128)(2,1)S(1)}, bf16[64,512]{1,0:T(8,128)(2,1)S(1)}, u32[]{:S(2)}, u32[]{:S(2)}) collective-permute-start(bf16[64,512]{1,0:T(8,128)(2,1)S(1)} %slice.206), channel_id=1, source_target_pairs={{0,6},{2,0},{4,2},{6,4},{1,7},{3,1},{5,3},{7,5},{8,14},{10,8},{12,... | collective-permute-start | bytes 196616 | tf_op jit(solution)/shard_map/ppermute | solution.py:49
  87.2 13.0 %copy-start = (f32[2,12,1,64,128]{4,3,2,1,0:T(8,128)S(1)}, f32[2,12,1,64,128]{4,3,2,1,0:T(8,128)}, u32[]{:S(2)}) copy-start(f32[2,12,1,64,128]{4,3,2,1,0:T(8,128)} %param.21) | copy-start | bytes 2359300
  87.7 13.1 %copy-start.3 = (bf16[2,128,512]{2,1,0:T(8,128)(2,1)S(1)}, bf16[2,128,512]{2,1,0:T(8,128)(2,1)}, u32[]{:S(2)}) copy-start(bf16[2,128,512]{2,1,0:T(8,128)(2,1)} %param.19) | copy-start | bytes 786436
  88.9 10.9 %all-to-all-start.1 = ((bf16[8,12,960]{2,1,0:T(8,128)(2,1)}), bf16[8,12,960]{2,1,0:T(8,128)(2,1)S(1)}, u32[]{:S(2)}, u32[]{:S(2)}) async-start(bf16[8,12,960]{2,1,0:T(8,128)(2,1)} %concatenate.46), calls=%async_computation.1 | async-start | bytes 524288 | tf_op jit(solution)/shard_map/all_to_all | solution.py:26
  92.7 8.4 %collective-permute-start.4 = (bf16[4,128,512]{2,1,0:T(8,128)(2,1)S(1)}, bf16[4,128,512]{2,1,0:T(8,128)(2,1)S(1)}, u32[]{:S(2)}, u32[]{:S(2)}) collective-permute-start(bf16[4,128,512]{2,1,0:T(8,128)(2,1)S(1)} %pad_maximum_fusion.2), channel_id=1, source_target_pairs={{0,1},{1,0},{2,3},{3,2},{4,5},{5,4},{6,7},{7,6},{8,9},{9,8},{10,11... | collective-permute-start | bytes 1572872 | tf_op jit(solution)/shard_map/ppermute | solution.py:62
  100.1 16.5 %copy-start.14 = (f32[12,128]{1,0:T(8,128)}, f32[12,128]{1,0:T(8,128)S(1)}, u32[]{:S(2)}) copy-start(f32[12,128]{1,0:T(8,128)S(1)} %slice.203) | copy-start | bytes 18436
  100.2 16.4 %copy-start.10 = (f32[12,64]{1,0:T(8,128)}, f32[12,64]{1,0:T(8,128)S(1)}, u32[]{:S(2)}) copy-start(f32[12,64]{1,0:T(8,128)S(1)} %get-tuple-element.28) | copy-start | bytes 9220
  100.2 16.4 %copy-start.12 = (f32[12,64]{1,0:T(8,128)}, f32[12,64]{1,0:T(8,128)S(1)}, u32[]{:S(2)}) copy-start(f32[12,64]{1,0:T(8,128)S(1)} %get-tuple-element.29) | copy-start | bytes 9220
  111.2 38.5 %all-to-all-start.3 = ((bf16[8,2,12,512]{3,1,2,0:T(2,128)(2,1)}), bf16[8,2,12,512]{3,1,2,0:T(2,128)(2,1)S(1)}, u32[]{:S(2)}, u32[]{:S(2)}) async-start(bf16[8,2,12,512]{3,1,2,0:T(2,128)(2,1)} %broadcast_in_dim.11), calls=%async_computation.3 | async-start | bytes 393216 | tf_op jit(solution)/shard_map/all_to_all | solution.py:26
  119.4 13.9 %collective-permute-start.5 = (bf16[464,512]{1,0:T(8,128)(2,1)S(1)}, bf16[464,512]{1,0:T(8,128)(2,1)S(1)}, u32[]{:S(2)}, u32[]{:S(2)}) collective-permute-start(bf16[464,512]{1,0:T(8,128)(2,1)S(1)} %concatenate.48), channel_id=1, source_target_pairs={{0,2},{2,4},{4,6},{6,0},{1,3},{3,5},{5,7},{7,1},{8,10},{10,12},{12... | collective-permute-start | bytes 1425416 | tf_op jit(solution)/shard_map/ppermute | solution.py:46
  122.0 13.4 %collective-permute-start.7 = (bf16[464,512]{1,0:T(8,128)(2,1)S(1)}, bf16[464,512]{1,0:T(8,128)(2,1)S(1)}, u32[]{:S(2)}, u32[]{:S(2)}) collective-permute-start(bf16[464,512]{1,0:T(8,128)(2,1)S(1)} %concatenate.48), channel_id=1, source_target_pairs={{0,6},{2,0},{4,2},{6,4},{1,7},{3,1},{5,3},{7,5},{8,14},{10,8},{12,... | collective-permute-start | bytes 1425416 | tf_op jit(solution)/shard_map/ppermute | solution.py:49
  133.4 11.9 %copy-start.1 = (bf16[464,512]{1,0:T(8,128)(2,1)}, bf16[464,512]{1,0:T(8,128)(2,1)S(1)}, u32[]{:S(2)}) copy-start(bf16[464,512]{1,0:T(8,128)(2,1)S(1)} %collective-permute-done.5) | copy-start | bytes 1425412
  133.4 9.3 %collective-permute-start.6 = (bf16[232,512]{1,0:T(8,128)(2,1)S(1)}, bf16[232,512]{1,0:T(8,128)(2,1)}, u32[]{:S(2)}, u32[]{:S(2)}) collective-permute-start(bf16[232,512]{1,0:T(8,128)(2,1)S(1)} %slice.212), channel_id=1, source_target_pairs={{0,2},{2,4},{4,6},{6,0},{1,3},{3,5},{5,7},{7,1},{8,10},{10,12},{12... | collective-permute-start | bytes 712712 | tf_op jit(solution)/shard_map/ppermute | solution.py:46
  135.4 9.9 %copy-start.2 = (bf16[464,512]{1,0:T(8,128)(2,1)}, bf16[464,512]{1,0:T(8,128)(2,1)S(1)}, u32[]{:S(2)}) copy-start(bf16[464,512]{1,0:T(8,128)(2,1)S(1)} %collective-permute-done.7) | copy-start | bytes 1425412
  135.4 8.8 %collective-permute-start.8 = (bf16[232,512]{1,0:T(8,128)(2,1)S(1)}, bf16[232,512]{1,0:T(8,128)(2,1)}, u32[]{:S(2)}, u32[]{:S(2)}) collective-permute-start(bf16[232,512]{1,0:T(8,128)(2,1)S(1)} %slice.213), channel_id=1, source_target_pairs={{0,6},{2,0},{4,2},{6,4},{1,7},{3,1},{5,3},{7,5},{8,14},{10,8},{12,... | collective-permute-start | bytes 712712 | tf_op jit(solution)/shard_map/ppermute | solution.py:49
  146.7 14.0 %collective-permute-start.9 = (bf16[4,464,512]{2,1,0:T(8,128)(2,1)S(1)}, bf16[4,464,512]{2,1,0:T(8,128)(2,1)}, u32[]{:S(2)}, u32[]{:S(2)}) collective-permute-start(bf16[4,464,512]{2,1,0:T(8,128)(2,1)S(1)} %pad_maximum_fusion), channel_id=1, source_target_pairs={{0,1},{1,0},{2,3},{3,2},{4,5},{5,4},{6,7},{7,6},{8,9},{9,8},{10,11... | collective-permute-start | bytes 5701640 | tf_op jit(solution)/shard_map/ppermute | solution.py:62
  150.6 9.2 %all-to-all-start.4 = ((bf16[4,2,12,512]{3,1,2,0:T(2,128)(2,1)}), bf16[4,2,12,512]{3,1,2,0:T(2,128)(2,1)S(1)}, u32[]{:S(2)}, u32[]{:S(2)}) async-start(bf16[4,2,12,512]{3,1,2,0:T(2,128)(2,1)} %broadcast_in_dim.12), calls=%async_computation.4 | async-start | bytes 196608 | tf_op jit(solution)/shard_map/all_to_all | solution.py:26
  163.6 11.1 %copy-start.4 = (bf16[2,128,512]{2,1,0:T(8,128)(2,1)S(1)}, bf16[2,128,512]{2,1,0:T(8,128)(2,1)}, u32[]{:S(2)}) copy-start(bf16[2,128,512]{2,1,0:T(8,128)(2,1)} %param.19) | copy-start | bytes 786436
  163.6 34.4 %copy-start.11 = (f32[12,64]{1,0:T(8,128)S(1)}, f32[12,64]{1,0:T(8,128)}, u32[]{:S(2)}) copy-start(f32[12,64]{1,0:T(8,128)} %copy-done.10) | copy-start | bytes 9220
  163.6 34.4 %copy-start.13 = (f32[12,64]{1,0:T(8,128)S(1)}, f32[12,64]{1,0:T(8,128)}, u32[]{:S(2)}) copy-start(f32[12,64]{1,0:T(8,128)} %copy-done.12) | copy-start | bytes 9220
  163.7 34.4 %copy-start.15 = (f32[12,128]{1,0:T(8,128)S(1)}, f32[12,128]{1,0:T(8,128)}, u32[]{:S(2)}) copy-start(f32[12,128]{1,0:T(8,128)} %copy-done.14) | copy-start | bytes 18436
  175.6 53.2 %all-to-all-start.6 = ((bf16[32,3,512]{2,1,0:T(4,128)(2,1)}), bf16[32,3,512]{2,1,0:T(4,128)(2,1)S(1)}, u32[]{:S(2)}, u32[]{:S(2)}) async-start(bf16[32,3,512]{2,1,0:T(4,128)(2,1)} %reshape.246), calls=%async_computation.6 | async-start | bytes 262144 | tf_op jit(solution)/shard_map/all_to_all | solution.py:26
  (2 other events, 6.1 us)
